TPU v7x, 32 devices: a whole 2x2x4 slice. The times are simulated.
32 devices in a mesh: ep: 8 (over z, x), tp: 4 (over y, core).
Axes of the slice: x: 2, y: 2, z: 4, core: 2. Of those that a mesh axis runs over, the one named last changes fastest.
Arguments:
- queries: bfloat16 [2048, 2, 1024], P('ep', None, 'tp')
- keys: bfloat16 [2048, 2, 256], P('ep', None, 'tp')
- values: bfloat16 [2048, 2, 256], P('ep', None, 'tp'), may hold values from -6 to 6
- query_gain: float32 [64], replicated, may hold values from 1.2 to 6
- key_gain: float32 [64], replicated, may hold values from 1.2 to 6
- out_weight: bfloat16 [1024, 2048], P('tp'), may hold values from -0.75 to 0.75
- moe_tokens: bfloat16 [4096, 2048], P(('ep', 'tp')), may hold values from -6 to 6
- moe_gain: float32 [2048], replicated, may hold values from 0.1 to 1.9
- routes: int32 [4096, 2], P(('ep', 'tp')), may hold values from 0 to 7, all different within a row; in each aligned block of 128 rows (0 to 127, 128 to 255, ...) at most 48 rows name the same one
- route_weight: float32 [4096, 2], P(('ep', 'tp')), may hold values from 0.1 to 1
- w_gate: bfloat16 [8, 2048, 1024], P('ep', None, 'tp'), may hold values from -0.125 to 0.125
- w_up: bfloat16 [8, 2048, 1024], P('ep', None, 'tp'), may hold values from -0.125 to 0.125
- w_down: bfloat16 [8, 1024, 2048], P('ep', 'tp'), may hold values from -0.1875 to 0.1875
Outputs:
- attended: bfloat16 [2048, 2, 2048], P(('ep', 'tp'))
- routed: bfloat16 [4096, 2048], P(('ep', 'tp'))
Inputs may be any that keep to these rules, and one draw needn't show every extreme that they name: `routes`: each row names 2 different experts. The rows of one device name no expert more than 48 times, and in every draw some device's rows name one expert exactly 48 times.
All inputs are finite; a program needn't handle non-finite values.
Results may differ from a plain program's by a relative error of at most 0.013.
The roundings to bfloat16 on the way count: a program that leaves them out, or rounds other values in their place, can miss the bound.
Values may be sent and summed in bfloat16 or wider, within the bound.
A program may use at most 128 MiB of HBM per device.

v0:
```python
import functools

import jax
import jax.numpy as jnp
from jax import lax
from jax.experimental import pallas as pl
from jax.experimental.pallas import tpu as pltpu
from jax.sharding import PartitionSpec as P

HEAD_DIM = 64
GRID_W = 64


EPS = 1e-06
THETA = 10000.0


def turn(normed, positions):
    quarter = normed.shape[-1] // 4
    inverse = THETA ** (-jnp.arange(quarter, dtype=jnp.float32) / quarter)
    grid_row = (positions // GRID_W).astype(jnp.float32)
    grid_col = (positions % GRID_W).astype(jnp.float32)
    angles = jnp.stack([grid_row[:, None] * inverse, grid_col[:, None] * inverse], axis=1)
    cosine = jnp.cos(angles)[:, None, None]
    sine = jnp.sin(angles)[:, None, None]
    parts = normed.reshape(normed.shape[:-1] + (2, 2, quarter))
    first = parts[..., 0, :]
    second = parts[..., 1, :]
    turned = jnp.stack([first * cosine - second * sine, second * cosine + first * sine], axis=-2)
    return turned.reshape(normed.shape)


def prepare(data, positions, gain):
    heads = data.astype(jnp.float32).reshape(data.shape[0], data.shape[1], -1, HEAD_DIM)
    normed = heads * lax.rsqrt(jnp.mean(heads * heads, axis=-1, keepdims=True) + EPS) * gain
    return turn(normed, positions).astype(jnp.bfloat16)


MESH = pl.DeviceIdType.MESH


def fused_kernel(experts, send, kv, q, out_weight, w_gate, w_up, w_down, ret, att, *scratch):
    (rows, kv_all, part, pair, gone, seen, done, prod, pair_att, gone_att, seen_att, packed, accum, best, total) = scratch[:15]
    (a_send, a_recv, y_send, y_recv, l_send, l_recv, m_send, m_recv, k_send, k_recv, x_send, x_recv) = scratch[15:27]
    (f_send, f_recv, n_send, n_recv, c_send, c_recv, b_send, b_recv, o_send, o_recv, own) = scratch[27:]
    f32, bf16 = jnp.float32, jnp.bfloat16
    e, t = lax.axis_index("ep"), lax.axis_index("tp")
    low, high = t + 1 - 2 * (t % 2), (t + 2) % 4
    low_high = (low + 2) % 4
    half = experts // 2
    side = e + 1 - 2 * (e % 2)
    capacity = send.shape[1]
    stride = packed.shape[0] // 4

    def remote(src, dst, s, r, device):
        return pltpu.make_async_remote_copy(
            src_ref=src, dst_ref=dst, send_sem=s, recv_sem=r, device_id=device, device_id_type=MESH
        )

    def source(k):
        return (e - k + experts) % experts

    def kv_direct(k):
        return remote(kv, kv_all.at[e], k_send.at[k], k_recv.at[k], ((e + 2 * k) % experts, t))

    def kv_side(k):
        block = kv_all.at[(e - 2 * k + experts) % experts]
        return remote(block, block, x_send.at[k], x_recv.at[k], (side, t))

    def chunk(k):
        return remote(send.at[(e + k) % experts], rows.at[t, e], a_send.at[k], a_recv.at[k], ((e + k) % experts, t))

    def across(k):
        block = rows.at[t, source(k)]
        return remote(block, block, y_send.at[k], y_recv.at[k], (e, high))

    def beside(k):
        block = rows.at[t, source(k)]
        return remote(block, block, l_send.at[k], l_recv.at[k], (e, low))

    def relay(k):
        block = rows.at[high, source(k)]
        return remote(block, block, m_send.at[k], m_recv.at[k], (e, low))

    def pair_far(k):
        return remote(part.at[low_high, k], pair.at[1, k], f_send.at[k], f_recv.at[k], (e, low))

    def pair_near(k):
        return remote(part.at[low, k], pair.at[0, k], n_send.at[k], n_recv.at[k], (e, low))

    def over(k):
        return remote(gone.at[k], seen.at[k], c_send.at[k], c_recv.at[k], (e, high))

    def back(k):
        return remote(done.at[k], ret.at[e], b_send.at[k], b_recv.at[k], (source(k), t))

    def other(i):
        if i < 2:
            return remote(prod.at[(low, low_high)[i]], pair_att.at[i], o_send.at[i], o_recv.at[i], (e, low))
        return remote(gone_att, seen_att, o_send.at[i], o_recv.at[i], (e, high))

    def attend(owner):
        for s in range(kv.shape[0]):
            block = kv_all[owner, s]
            scores = lax.dot_general(block, q[s], (((1,), (1,)), ((), ())), preferred_element_type=f32)
            old = best[s]
            new = jnp.maximum(old, jnp.max(scores, axis=0, keepdims=True))
            factor = jnp.exp(old - new)
            expo = jnp.exp(scores - new)
            best[s] = new
            total[s] = total[s] * factor + jnp.sum(expo, axis=0, keepdims=True)
            added = lax.dot_general(block, expo.astype(bf16), (((0,), (0,)), ((), ())), preferred_element_type=f32)
            accum[s] = accum[s] * factor + added

    def project():
        positions = kv.shape[1]
        quarter = positions // 4
        for s in range(kv.shape[0]):
            mixed = (accum[s, HEAD_DIM:, :] / total[s]).astype(bf16)
            groups = mixed.shape[1] // positions
            stacked = jnp.concatenate([mixed[:, g * positions : (g + 1) * positions] for g in range(groups)], axis=0)
            product = lax.dot_general(stacked, out_weight[...], (((0,), (0,)), ((), ())), preferred_element_type=f32)
            product = product.astype(bf16)
            for b in range(4):
                prod[b, s * quarter : (s + 1) * quarter, :] = product[b * quarter : (b + 1) * quarter]

    def expert(k):
        for b in range(4):
            packed[b * stride : b * stride + capacity, :] = rows[b, source(k)]
        data = packed[...]
        gate = jnp.dot(data, w_gate[...], preferred_element_type=f32)
        up = jnp.dot(data, w_up[...], preferred_element_type=f32)
        hidden = (gate * (1.0 / (1.0 + jnp.exp(-gate))) * up).astype(bf16)
        result = jnp.dot(hidden, w_down[...], preferred_element_type=f32).astype(bf16)
        for b in range(4):
            part[b, k] = result[b * stride : b * stride + capacity]

    barrier = pltpu.get_barrier_semaphore()
    partners = [((e + k) % experts, t) for k in range(1, experts)] + [(e, low), (e, high)]
    for device in partners:
        pl.semaphore_signal(barrier, inc=1, device_id=device, device_id_type=MESH)
    pl.semaphore_wait(barrier, len(partners))

    own_chunk = pltpu.make_async_copy(send.at[e], rows.at[t, e], own.at[0])
    own_chunk.start()
    own_kv = pltpu.make_async_copy(kv, kv_all.at[e], own.at[1])
    own_kv.start()
    lax.fori_loop(1, experts, lambda k, c: (chunk(k).start(), c)[1], 0)
    lax.fori_loop(1, half, lambda k, c: (kv_direct(k).start(), c)[1], 0)
    best[...] = jnp.full_like(best, -1e30)
    total[...] = jnp.zeros_like(total)
    accum[...] = jnp.zeros_like(accum)
    own_chunk.wait()
    own_kv.wait()
    kv_side(0).start()

    def step(k, carry):
        @pl.when((k >= 1) & (k < experts))
        def _():
            chunk(k).wait_recv()

        @pl.when(k < experts)
        def _():
            across(k).start()
            beside(k).start()

        @pl.when((k >= 2) & (k < experts + 2))
        def _():
            across(k - 2).wait_recv()
            relay(k - 2).start()

        @pl.when((k >= 4) & (k < experts + 4))
        def _():
            pair_far(k - 4).start()
            pair_near(k - 4).start()

        @pl.when((k >= 3) & (k < experts + 3))
        def _():
            beside(k - 3).wait_recv()
            relay(k - 3).wait_recv()
            expert(k - 3)

        @pl.when((k >= 6) & (k < experts + 6))
        def _():
            over(k - 6).start()

        @pl.when((k >= 5) & (k < experts + 5))
        def _():
            j = k - 5
            pair_far(j).wait_recv()
            gone[j] = (part[high, j].astype(f32) + pair[1, j].astype(f32)).astype(bf16)

        @pl.when(k == experts + 7)
        def _():
            other(1).wait_recv()
            gone_att[...] = (prod[high].astype(f32) + pair_att[1].astype(f32)).astype(bf16)

        @pl.when(k == experts + 9)
        def _():
            other(2).start()

        @pl.when(k == 10)
        def _():
            pltpu.make_async_copy(done.at[0], ret.at[e], own.at[0]).start()

        @pl.when((k >= 11) & (k < experts + 10))
        def _():
            back(k - 10).start()

        @pl.when((k >= 9) & (k < experts + 9))
        def _():
            j = k - 9
            pair_near(j).wait_recv()
            over(j).wait_recv()
            done[j] = (part[t, j].astype(f32) + pair[0, j].astype(f32) + seen[j].astype(f32)).astype(bf16)

        @pl.when((k >= 6) & (k < half + 5))
        def _():
            kv_direct(k - 5).wait_recv()
            kv_side(k - 5).start()

        @pl.when((k >= half + 5) & (k < experts + 5))
        def _():
            kv_side(k - 5 - half).wait_recv()

        @pl.when((k >= 5) & (k < experts + 5))
        def _():
            i = k - 5
            direct = (e - 2 * i + 2 * experts) % experts
            beyond = (side - 2 * (i - half) + 2 * experts) % experts
            near = (experts + half - 1 - i) // experts
            attend(near * direct + (1 - near) * beyond)

        @pl.when(k == experts + 5)
        def _():
            project()

        @pl.when(k == experts + 6)
        def _():
            other(1).start()
            other(0).start()

        return carry

    lax.fori_loop(0, experts + 10, step, 0)
    other(0).wait_recv()
    other(2).wait_recv()
    att[...] = (prod[t].astype(f32) + pair_att[0].astype(f32) + seen_att[...].astype(f32)).astype(bf16)

    def finish(k, carry):
        across(k).wait_send()
        beside(k).wait_send()
        relay(k).wait_send()
        pair_far(k).wait_send()
        pair_near(k).wait_send()
        over(k).wait_send()

        @pl.when(k >= 1)
        def _():
            chunk(k).wait_send()
            back(k).wait()

        @pl.when(k < half)
        def _():
            kv_side(k).wait_send()

        @pl.when((k >= 1) & (k < half))
        def _():
            kv_direct(k).wait_send()

        return carry

    lax.fori_loop(0, experts, finish, 0)
    for i in range(3):
        other(i).wait_send()
    pltpu.make_async_copy(done.at[0], ret.at[e], own.at[0]).wait()


def fused(experts, send, kv, q, out_weight, w_gate, w_up, w_down):
    sem = pltpu.SemaphoreType.DMA((experts,))
    like = send.dtype
    capacity, features = send.shape[1:]
    seqs, positions, lanes = kv.shape
    att = (positions // 4 * seqs, features)
    queries = q.shape[1]
    stride = -(-capacity // 16) * 16
    shapes = [
        (4,) + send.shape,
        (experts,) + kv.shape,
        (4,) + send.shape,
        (2,) + send.shape,
        send.shape,
        send.shape,
        send.shape,
        (4,) + att,
        (2,) + att,
        att,
        att,
        (4 * stride, features),
    ]
    vmem = pl.BlockSpec(memory_space=pltpu.VMEM)
    return pl.pallas_call(
        functools.partial(fused_kernel, experts),
        out_shape=(jax.ShapeDtypeStruct(send.shape, like), jax.ShapeDtypeStruct(att, like)),
        in_specs=[vmem] * 7,
        out_specs=(vmem, vmem),
        scratch_shapes=[pltpu.VMEM(shape, like) for shape in shapes]
        + [
            pltpu.VMEM((seqs, lanes, queries), jnp.float32),
            pltpu.VMEM((seqs, 1, queries), jnp.float32),
            pltpu.VMEM((seqs, 1, queries), jnp.float32),
        ]
        + [sem] * 20
        + [pltpu.SemaphoreType.DMA((3,))] * 2
        + [pltpu.SemaphoreType.DMA((2,))],
        name="fused",
        compiler_params=pltpu.CompilerParams(
            collective_id=1, has_side_effects=True, vmem_limit_bytes=62 * 2**20
        ),
    )(send, kv, q, out_weight, w_gate, w_up, w_down)


def per_device(
    queries,
    keys,
    values,
    query_gain,
    key_gain,
    out_weight,
    moe_tokens,
    moe_gain,
    routes,
    route_weight,
    w_gate,
    w_up,
    w_down,
):
    pos_count = queries.shape[0]
    seq_count = queries.shape[1]
    positions = lax.axis_index("ep") * pos_count + jnp.arange(pos_count, dtype=jnp.int32)
    q_rot = prepare(queries, positions, query_gain)
    k_rot = prepare(keys, positions, key_gain)
    kv_local = k_rot.shape[2]
    groups = q_rot.shape[2] // kv_local
    value_heads = values.reshape(pos_count, seq_count, kv_local, HEAD_DIM)
    q_group = q_rot.reshape(pos_count, seq_count, kv_local, groups, HEAD_DIM)
    scale = HEAD_DIM ** (-0.5)
    tok_count = moe_tokens.shape[0]
    top_count = routes.shape[1]
    experts = lax.axis_size("ep")
    capacity = max(2, (3 * tok_count * top_count + 2 * experts - 1) // (2 * experts))
    token_float = moe_tokens.astype(jnp.float32)
    normed = (
        token_float
        * lax.rsqrt(jnp.mean(token_float * token_float, axis=-1, keepdims=True) + EPS)
        * moe_gain
    ).astype(jnp.bfloat16)
    hits = (routes[:, :, None] == jnp.arange(experts, dtype=jnp.int32)[None, None, :]).astype(
        jnp.float32
    )
    pair_count = tok_count * top_count
    flat_hits = hits.reshape(pair_count, experts)
    pair_index = jnp.arange(pair_count, dtype=jnp.int32)
    earlier = (pair_index[:, None] > pair_index[None, :]).astype(jnp.float32)
    before = jnp.dot(earlier, flat_hits, precision=lax.Precision.HIGHEST)
    rank = jnp.sum(before * flat_hits, axis=-1).astype(jnp.int32).reshape(tok_count, top_count)
    slot = routes * capacity + rank
    table = jnp.arange(experts * capacity, dtype=jnp.int32)
    dispatch = jnp.sum(
        (slot[None, :, :] == table[:, None, None]).astype(jnp.float32), axis=2
    ).astype(jnp.bfloat16)
    send = jnp.dot(dispatch, normed, preferred_element_type=jnp.float32).astype(jnp.bfloat16)
    kv = jnp.concatenate([k_rot, value_heads], axis=-1)
    kv = jnp.transpose(kv, (1, 2, 0, 3)).reshape(seq_count * kv_local, pos_count, 2 * HEAD_DIM)
    q_rows = jnp.transpose(q_group * jnp.bfloat16(scale), (1, 2, 3, 0, 4))
    q_rows = jnp.pad(q_rows, ((0, 0),) * 4 + ((0, HEAD_DIM),))
    q_rows = q_rows.reshape(seq_count * kv_local, groups * pos_count, 2 * HEAD_DIM)
    returned_rows, attended = fused(
        experts,
        send.reshape(experts, capacity, -1),
        kv,
        q_rows,
        out_weight,
        w_gate[0],
        w_up[0],
        w_down[0],
    )
    returned_rows = returned_rows.reshape(experts * capacity, -1)
    quarter = pos_count // lax.axis_size("tp")
    attended = jnp.transpose(attended.reshape(seq_count, quarter, -1), (1, 0, 2))
    combined = jnp.zeros((tok_count, returned_rows.shape[-1]), jnp.float32)
    for choice_index in range(top_count):
        picker = (slot[:, choice_index : choice_index + 1] == table[None, :]).astype(jnp.bfloat16)
        picked = jnp.dot(picker, returned_rows, preferred_element_type=jnp.float32)
        combined = combined + picked * route_weight[:, choice_index : choice_index + 1]
    return (attended, combined.astype(jnp.bfloat16))


def solution(mesh):
    in_specs = (
        P("ep", None, "tp"),
        P("ep", None, "tp"),
        P("ep", None, "tp"),
        P(),
        P(),
        P("tp", None),
        P(("ep", "tp"), None),
        P(),
        P(("ep", "tp"), None),
        P(("ep", "tp"), None),
        P("ep", None, "tp"),
        P("ep", None, "tp"),
        P("ep", "tp", None),
    )
    out_specs = (P(("ep", "tp"), None, None), P(("ep", "tp"), None))
    return jax.shard_map(
        per_device, mesh=mesh, in_specs=in_specs, out_specs=out_specs, check_vma=False
    )
```

profile of v0, /device:TPU:0, one launch (start us, length us, event | category | flops | bytes accessed | tf_op | source)
XLA Modules:
  0.0 127.9 jit_solution(1512589419353581769)
XLA Ops:
  0.7 0.1 broadcast_multiply_fusion.1
  0.7 0.1 fusion.15
  0.9 1.1 copy.50
  2.0 0.1 bitcast_reduce_fusion
  2.1 0.7 mul.271
  2.8 0.1 multiply_multiply_fusion
  2.9 0.0 copy-start.3
  2.9 0.0 copy-start.8
  3.0 0.1 subtract_convert_fusion
  3.0 0.0 copy-start.4
  3.1 0.0 copy-start.6
  3.1 0.3 copy.53
  3.4 0.0 copy-start.1
  3.4 0.0 copy-start.5
  3.4 0.9 pad.4.clone
  4.3 0.0 copy-done.3
  4.4 0.0 copy-done.8
  4.4 0.1 fusion.10
  4.5 0.1 copy.49
  4.6 0.0 copy-done.4
  4.6 0.1 copy.48
  4.8 0.8 maximum_bitcast_fusion.kv
  5.5 0.0 copy-done.6
  5.5 0.1 copy.46
  5.7 0.1 eq.63
  5.8 0.2 fusion.2
  6.0 0.1 convert_element_type.76
  6.2 0.1 copy.47
  6.2 0.1 convert_reduce_fusion
  6.3 0.0 copy-done.1
  6.3 0.2 fusion.3
  6.5 0.0 copy-done.5
  6.5 1.8 %convolution_convert_fusion = bf16[384,2048]{1,0:T(8,128)(2,1)} fusion(bf16[128,2048]{1,0:T(8,128)(2,1)S(1)} %copy-done.1, f32[2048]{0:T(1024)S(1)} %copy-done.5, f32[128]{0:T(128)S(1)} %add_rsqrt_fusion.2, bf16[384,128]{1,0:T(8,128)(2,1)S(1)} %convert_reduce_fusion), kind=kOutput, calls=%fused_computation | convolution fusion | flops 203161600 | bytes 2204160 | tf_op jit(solution)/shard_map/dot_general | solution.py:372
  8.3 0.0 copy-start.7
  8.3 114.8 %fused.1 = (bf16[8,48,2048]{2,1,0:T(8,128)(2,1)}, bf16[128,2048]{1,0:T(8,128)(2,1)}) custom-call(bf16[8,48,2048]{2,1,0:T(8,128)(2,1)} %bitcast.37, bf16[2,256,128]{2,1,0:T(8,128)(2,1)} %maximum_bitcast_fusion.kv, bf16[2,1024,128]{2,1,0:T(8,128)(2,1)} %bitcast.39, bf16[256,2048]{1,0:T(8,128)(2,1)} %out_weight.1, bf16[2048,256]{1,0:T(8,128)(2,1)} %bitcast.40, ...), custom_call_target="tpu_custom_call" | custom-call | tf_op jit(solution)/shard_map/fused/pallas_call | solution.py:302
  123.2 0.0 copy-start
  123.2 0.0 copy-done.7
  123.2 2.0 %convolution_multiply_fusion.1 = f32[128,2048]{1,0:T(8,128)S(1)} fusion(bf16[384,2048]{1,0:T(8,128)(2,1)} %bitcast.35, f32[128]{0:T(128)S(1)} %get-tuple-element.15, s32[128]{0:T(128)S(1)} %get-tuple-element.13), kind=kOutput, calls=%fused_computation.3 | convolution fusion | flops 201637888 | bytes 2622464 | tf_op jit(solution)/shard_map/dot_general | solution.py:394
  125.2 0.0 copy-done
  125.2 0.0 copy-start.2
  125.2 1.3 %fusion.1 = bf16[128,2048]{1,0:T(8,128)(2,1)} fusion(f32[128,2048]{1,0:T(8,128)S(1)} %convolution_multiply_fusion.1, bf16[384,2048]{1,0:T(8,128)(2,1)S(1)} %bitcast.36, f32[128]{0:T(128)S(1)} %get-tuple-element.14, s32[128]{0:T(128)S(1)} %get-tuple-element.12), kind=kOutput, calls=%fused_computation.4 | convolution fusion | flops 202162176 | bytes 3146752 | tf_op jit(solution)/shard_map/dot_general | solution.py:394
  126.5 0.0 copy-done.2
  126.5 1.3 %copy.55 = bf16[2,64,2048]{2,0,1:T(2,128)(2,1)} copy(bf16[2,64,2048]{2,1,0:T(8,128)(2,1)S(1)} %bitcast.45) | data formatting | bytes 1048576 | tf_op jit(solution)/shard_map/reshape | solution.py:390
  (13 shorter events, 0.2 us)
Async XLA Ops:
  2.9 1.4 %copy-start.3 = (bf16[256,2,64]{0,2,1:T(8,128)(2,1)S(1)}, bf16[256,2,64]{0,2,1:T(8,128)(2,1)}, u32[]{:S(2)}) copy-start(bf16[256,2,64]{0,2,1:T(8,128)(2,1)} %param.14) | copy-start | bytes 196612
  2.9 1.4 %copy-start.8 = (f32[64]{0:T(128)S(1)}, f32[64]{0:T(128)}, u32[]{:S(2)}) copy-start(f32[64]{0:T(128)} %param.17) | copy-start | bytes 772
  3.0 1.6 %copy-start.4 = (bf16[256,2,64]{0,2,1:T(8,128)(2,1)S(1)}, bf16[256,2,64]{0,2,1:T(8,128)(2,1)}, u32[]{:S(2)}) copy-start(bf16[256,2,64]{0,2,1:T(8,128)(2,1)} %param.15) | copy-start | bytes 196612
  3.1 2.4 %copy-start.6 = (s32[128,2]{0,1:T(2,128)S(1)}, s32[128,2]{0,1:T(2,128)}, u32[]{:S(2)}) copy-start(s32[128,2]{0,1:T(2,128)} %param.21) | copy-start | bytes 3076
  3.4 2.9 %copy-start.1 = (bf16[128,2048]{1,0:T(8,128)(2,1)S(1)}, bf16[128,2048]{1,0:T(8,128)(2,1)}, u32[]{:S(2)}) copy-start(bf16[128,2048]{1,0:T(8,128)(2,1)} %param.19) | copy-start | bytes 1572868
  3.4 3.1 %copy-start.5 = (f32[2048]{0:T(1024)S(1)}, f32[2048]{0:T(1024)}, u32[]{:S(2)}) copy-start(f32[2048]{0:T(1024)} %param.20) | copy-start | bytes 24580
  8.3 114.8 %copy-start.7 = (f32[128,2]{0,1:T(2,128)S(1)}, f32[128,2]{0,1:T(2,128)}, u32[]{:S(2)}) copy-start(f32[128,2]{0,1:T(2,128)} %param.22) | copy-start | bytes 3076
  123.2 2.1 %copy-start = (bf16[8,48,2048]{2,1,0:T(8,128)(2,1)S(1)}, bf16[8,48,2048]{2,1,0:T(8,128)(2,1)}, u32[]{:S(2)}) copy-start(bf16[8,48,2048]{2,1,0:T(8,128)(2,1)} %get-tuple-element.5) | copy-start | bytes 4718596
  125.2 1.3 %copy-start.2 = (bf16[128,2048]{1,0:T(8,128)(2,1)S(1)}, bf16[128,2048]{1,0:T(8,128)(2,1)}, u32[]{:S(2)}) copy-start(bf16[128,2048]{1,0:T(8,128)(2,1)} %get-tuple-element.4) | copy-start | bytes 1572868
where the time goes:
time: 128 us
  Pallas kernels  115 us (90%)
  matrix products  5.33 us (4%)
  local copies, waits for them, and re-layouts  5.09 us (4%)
  other arithmetic  1.74 us (1%)
    pallas_call x1, Pallas kernels, fused(): pl.pallas_call(functools.partial(fused_kernel, experts), out_shape=(jax.S...  115 us
    dot_general x2, matrix products, per_device(): picked = jnp.dot(picker, returned_rows, preferred_element_type=jnp.float32)  3.3 us

commit v1 on v0

v1 whole, which is shorter than its diff:
```python
import functools
import math

import jax
import jax.numpy as jnp
from jax import lax
from jax.experimental import pallas as pl
from jax.experimental.pallas import tpu as pltpu
from jax.sharding import PartitionSpec as P

HEAD_DIM = 64
QUARTER = HEAD_DIM // 4
GRID_W = 64

EPS = 1e-06
THETA = 10000.0

MESH = pl.DeviceIdType.MESH


def exclusive_or(a, b, count):
    result = 0
    bit = 1
    while bit < count:
        result = result + (a // bit + b // bit) % 2 * bit
        bit *= 2
    return result


def turned(block, gain, cosine, sine):
    block = block.astype(jnp.float32)
    mean = jnp.mean(block * block, axis=0, keepdims=True)
    normed = block * lax.rsqrt(mean + EPS) * gain
    parts = []
    for axis in range(2):
        first = normed[2 * axis * QUARTER : (2 * axis + 1) * QUARTER]
        second = normed[(2 * axis + 1) * QUARTER : (2 * axis + 2) * QUARTER]
        c = cosine[axis * QUARTER : (axis + 1) * QUARTER]
        s = sine[axis * QUARTER : (axis + 1) * QUARTER]
        parts += [first * c - second * s, second * c + first * s]
    return jnp.concatenate(parts, axis=0).astype(jnp.bfloat16)


def fused_kernel(
    experts, capacity, tokens, moe_gain, routes, weights, queries, keys, values, q_gain, k_gain, cosine, sine,
    out_weight_hbm, w_gate_hbm, w_up_hbm, w_down_hbm, routed, att, *scratch
):
    (send, rows, part, pair, gone, seen, done, ret, packed, normed) = scratch[:10]
    (kv_all, q, prod, pair_att, gone_att, seen_att, accum, best, total, codes, combined) = scratch[10:21]
    (out_weight, w_gate, w_up, w_down, w_sem, own) = scratch[21:27]
    (a_send, a_recv, y_send, y_recv, l_send, l_recv, m_send, m_recv, k_send, k_recv, x_send, x_recv) = scratch[27:39]
    (f_send, f_recv, n_send, n_recv, c_send, c_recv, b_send, b_recv, o_send, o_recv) = scratch[39:]
    f32, bf16 = jnp.float32, jnp.bfloat16
    e, t = lax.axis_index("ep"), lax.axis_index("tp")
    low, high = t + 1 - 2 * (t % 2), (t + 2) % 4
    low_high = (low + 2) % 4
    half = experts // 2
    side = e + 1 - 2 * (e % 2)
    stride = packed.shape[0] // 4
    streams = kv_all.shape[1]
    positions = kv_all.shape[3]
    groups = q.shape[2] // positions
    tok_count = tokens.shape[0]

    def peer(k):
        return exclusive_or(e, k, experts)

    def remote(src, dst, s, r, device):
        return pltpu.make_async_remote_copy(
            src_ref=src, dst_ref=dst, send_sem=s, recv_sem=r, device_id=device, device_id_type=MESH
        )

    def kv_direct(m):
        return remote(kv_all.at[0], kv_all.at[2 * m], k_send.at[m], k_recv.at[m], (peer(2 * m), t))

    def kv_side(m):
        return remote(kv_all.at[2 * m], kv_all.at[2 * m + 1], x_send.at[m], x_recv.at[m], (side, t))

    def chunk(k):
        return remote(send.at[k], rows.at[t, k], a_send.at[k], a_recv.at[k], (peer(k), t))

    def across(k):
        block = rows.at[t, k]
        return remote(block, block, y_send.at[k], y_recv.at[k], (e, high))

    def beside(k):
        block = rows.at[t, k]
        return remote(block, block, l_send.at[k], l_recv.at[k], (e, low))

    def relay(k):
        block = rows.at[high, k]
        return remote(block, block, m_send.at[k], m_recv.at[k], (e, low))

    def pair_far(k):
        return remote(part.at[low_high, k], pair.at[1, k], f_send.at[k], f_recv.at[k], (e, low))

    def pair_near(k):
        return remote(part.at[low, k], pair.at[0, k], n_send.at[k], n_recv.at[k], (e, low))

    def over(k):
        return remote(gone.at[k], seen.at[k], c_send.at[k], c_recv.at[k], (e, high))

    def back(k):
        return remote(done.at[k], ret.at[k], b_send.at[k], b_recv.at[k], (peer(k), t))

    def other(i):
        if i < 2:
            return remote(prod.at[(low, low_high)[i]], pair_att.at[i], o_send.at[i], o_recv.at[i], (e, low))
        return remote(gone_att, seen_att, o_send.at[i], o_recv.at[i], (e, high))

    def own_copy(i):
        if i == 0:
            return pltpu.make_async_copy(send.at[0], rows.at[t, 0], own.at[0])
        return pltpu.make_async_copy(done.at[0], ret.at[0], own.at[1])

    def weight_copy(i):
        pairs = ((out_weight_hbm, out_weight), (w_gate_hbm, w_gate), (w_up_hbm, w_up), (w_down_hbm, w_down))
        return pltpu.make_async_copy(pairs[i][0], pairs[i][1], w_sem.at[i])

    def attend(j):
        for s in range(streams):
            key_block = kv_all[j, s, :HEAD_DIM]
            value_block = kv_all[j, s, HEAD_DIM:]
            scores = lax.dot_general(key_block, q[s], (((0,), (0,)), ((), ())), preferred_element_type=f32)
            old = best[s]
            new = jnp.maximum(old, jnp.max(scores, axis=0, keepdims=True))
            factor = jnp.exp(old - new)
            expo = jnp.exp(scores - new)
            best[s] = new
            total[s] = total[s] * factor + jnp.sum(expo, axis=0, keepdims=True)
            added = jnp.dot(value_block, expo.astype(bf16), preferred_element_type=f32)
            accum[s] = accum[s] * factor + added

    def project():
        quarter = positions // 4
        for s in range(streams):
            mixed = (accum[s] / total[s]).astype(bf16)
            stacked = jnp.concatenate([mixed[:, g * positions : (g + 1) * positions] for g in range(groups)], axis=0)
            product = lax.dot_general(stacked, out_weight[...], (((0,), (0,)), ((), ())), preferred_element_type=f32)
            product = product.astype(bf16)
            for b in range(4):
                prod[b, s * quarter : (s + 1) * quarter, :] = product[b * quarter : (b + 1) * quarter]

    def expert(k):
        for b in range(4):
            packed[b * stride : b * stride + capacity, :] = rows[b, k]
        data = packed[...]
        gate = jnp.dot(data, w_gate[...], preferred_element_type=f32)
        up = jnp.dot(data, w_up[...], preferred_element_type=f32)
        hidden = (gate * (1.0 / (1.0 + jnp.exp(-gate))) * up).astype(bf16)
        result = jnp.dot(hidden, w_down[...], preferred_element_type=f32).astype(bf16)
        for b in range(4):
            part[b, k] = result[b * stride : b * stride + capacity]

    def places(k):
        row = codes[pl.ds(peer(k), 1), :]
        slot = lax.broadcasted_iota(jnp.int32, (stride, tok_count), 0).astype(f32)
        return (slot == row).astype(f32)

    batch = min(experts, 4)

    def dispatch(g):
        table = jnp.concatenate([places(g * batch + i) for i in range(batch)], axis=0).astype(bf16)
        chosen = jnp.dot(table, normed[...], preferred_element_type=f32).astype(bf16)
        for i in range(batch):
            send[g * batch + i] = chosen[i * stride : i * stride + capacity]

    def send_batch(g):
        for i in range(batch):
            if i == 0:

                @pl.when(g > 0)
                def _():
                    chunk(g * batch).start()
            else:
                chunk(g * batch + i).start()

    def column(row):
        square = (tok_count, tok_count)
        diagonal = lax.broadcasted_iota(jnp.int32, square, 0) == lax.broadcasted_iota(jnp.int32, square, 1)
        return jnp.sum(jnp.where(diagonal, row, 0.0), axis=1, keepdims=True)

    def combine(k):
        if stride == capacity:
            data = ret[k]
        else:
            packed[:capacity, :] = ret[k]
            data = packed[:stride]
        table = places(k)
        picked = lax.dot_general(table.astype(bf16), data, (((0,), (0,)), ((), ())), preferred_element_type=f32)
        expert_id = peer(k)
        weight_row = jnp.zeros((1, tok_count), f32)
        for c in range(routes.shape[0]):
            weight_row = weight_row + jnp.where(routes[c : c + 1] == expert_id, weights[c : c + 1], 0.0)
        combined[...] += picked * column(weight_row)

    for i in range(4):
        weight_copy(i).start()
    barrier = pltpu.get_barrier_semaphore()
    partners = [(peer(k), t) for k in range(1, experts)] + [(e, low), (e, high)]
    for device in partners:
        pl.semaphore_signal(barrier, inc=1, device_id=device, device_id_type=MESH)

    for s in range(streams):
        kv_all[0, s, :HEAD_DIM] = turned(keys[s], k_gain[...], cosine[...], sine[...])
        kv_all[0, s, HEAD_DIM:] = values[s]

    if stride != capacity:
        packed[...] = jnp.zeros_like(packed)
    hits = jnp.zeros((experts, tok_count), f32)
    for c in range(routes.shape[0]):
        named = lax.broadcasted_iota(jnp.int32, (experts, tok_count), 0) == routes[c : c + 1]
        hits = hits + named.astype(f32)
    square = (tok_count, tok_count)
    earlier = lax.broadcasted_iota(jnp.int32, square, 0) < lax.broadcasted_iota(jnp.int32, square, 1)
    rank = jnp.dot(hits.astype(bf16), earlier.astype(f32).astype(bf16), preferred_element_type=f32)
    codes[...] = jnp.where(hits > 0.0, rank, -1.0)
    token_float = tokens[...].astype(f32)
    mean = jnp.mean(token_float * token_float, axis=-1, keepdims=True)
    normed[...] = (token_float * lax.rsqrt(mean + EPS) * moe_gain[...]).astype(bf16)

    pl.semaphore_wait(barrier, len(partners))

    lax.fori_loop(1, half, lambda m, c: (kv_direct(m).start(), c)[1], 0)
    kv_side(0).start()

    def dispatch_step(g, carry):
        @pl.when(g < experts // batch)
        def _():
            dispatch(g)

        @pl.when(g > 0)
        def _():
            send_batch(g - 1)

        @pl.when(g == experts // batch - 1)
        def _():
            for s in range(streams):
                for h in range(groups):
                    head = turned(queries[s, h * HEAD_DIM : (h + 1) * HEAD_DIM], q_gain[...], cosine[...], sine[...])
                    q[s, :, h * positions : (h + 1) * positions] = head * bf16(HEAD_DIM**-0.5)

        @pl.when(g == 1)
        def _():
            own_copy(0).start()

        return carry

    lax.fori_loop(0, experts // batch + 1, dispatch_step, 0)
    best[...] = jnp.full_like(best, -1e30)
    total[...] = jnp.zeros_like(total)
    accum[...] = jnp.zeros_like(accum)
    combined[...] = jnp.zeros_like(combined)
    own_copy(0).wait()
    across(0).start()
    beside(0).start()

    early = 2

    def attention_step(m, carry):
        attend(2 * m)

        @pl.when(m + 1 < half)
        def _():
            kv_direct(m + 1).wait_recv()
            kv_side(m + 1).start()

        kv_side(m).wait_recv()
        attend(2 * m + 1)

        @pl.when(m == half - 3)
        def _():
            chunk(1).wait_recv()
            across(1).start()
            beside(1).start()

        return carry

    lax.fori_loop(0, half, attention_step, 0)
    weight_copy(0).wait()
    project()
    for i in range(1, 4):
        weight_copy(i).wait()

    def step(k, carry):
        @pl.when((k >= early) & (k < experts))
        def _():
            chunk(k).wait_recv()
            across(k).start()
            beside(k).start()

        @pl.when((k >= 3) & (k < experts + 3))
        def _():
            pair_far(k - 3).start()
            pair_near(k - 3).start()

        @pl.when((k >= 5) & (k < experts + 5))
        def _():
            over(k - 5).start()

        @pl.when((k >= 8) & (k < experts + 7))
        def _():
            back(k - 7).start()

        @pl.when(k == 7)
        def _():
            own_copy(1).start()

        @pl.when(k == 1)
        def _():
            other(1).start()
            other(0).start()

        @pl.when((k >= 1) & (k < experts + 1))
        def _():
            across(k - 1).wait_recv()
            relay(k - 1).start()

        @pl.when(k == 3)
        def _():
            other(2).start()

        @pl.when((k >= 2) & (k < experts + 2))
        def _():
            beside(k - 2).wait_recv()
            relay(k - 2).wait_recv()
            expert(k - 2)

        @pl.when(k == 2)
        def _():
            other(1).wait_recv()
            gone_att[...] = (prod[high].astype(f32) + pair_att[1].astype(f32)).astype(bf16)

        @pl.when((k >= 4) & (k < experts + 4))
        def _():
            j = k - 4
            pair_far(j).wait_recv()
            gone[j] = (part[high, j].astype(f32) + pair[1, j].astype(f32)).astype(bf16)

        @pl.when((k >= 6) & (k < experts + 6))
        def _():
            j = k - 6
            pair_near(j).wait_recv()
            over(j).wait_recv()
            done[j] = (part[t, j].astype(f32) + pair[0, j].astype(f32) + seen[j].astype(f32)).astype(bf16)

        @pl.when((k >= 10) & (k < experts + 9))
        def _():
            back(k - 9).wait_recv()
            combine(k - 9)

        @pl.when(k == 9)
        def _():
            own_copy(1).wait()
            combine(0)

        @pl.when(k == experts + 1)
        def _():
            other(0).wait_recv()
            other(2).wait_recv()
            att[...] = (prod[t].astype(f32) + pair_att[0].astype(f32) + seen_att[...].astype(f32)).astype(bf16)

        return carry

    lax.fori_loop(0, experts + 9, step, 0)
    routed[...] = combined[...].astype(bf16)

    def finish(k, carry):
        across(k).wait_send()
        beside(k).wait_send()
        relay(k).wait_send()
        pair_far(k).wait_send()
        pair_near(k).wait_send()
        over(k).wait_send()

        @pl.when(k >= 1)
        def _():
            chunk(k).wait_send()
            back(k).wait_send()

        @pl.when(k < half)
        def _():
            kv_side(k).wait_send()

        @pl.when((k >= 1) & (k < half))
        def _():
            kv_direct(k).wait_send()

        return carry

    lax.fori_loop(0, experts, finish, 0)
    for i in range(3):
        other(i).wait_send()


def fused(experts, capacity, tokens, moe_gain, routes, weights, queries, keys, *rest):
    values, q_gain, k_gain, cosine, sine, out_weight, w_gate, w_up, w_down = rest
    like = tokens.dtype
    f32 = jnp.float32
    sem = pltpu.SemaphoreType.DMA((experts,))
    tok_count, features = tokens.shape
    streams, _, positions = keys.shape
    query_lanes = queries.shape[1] // HEAD_DIM * positions
    att = (positions // 4 * streams, features)
    stride = -(-capacity // 16) * 16
    block = (experts, capacity, features)
    shapes = [
        (block, like),
        ((4,) + block, like),
        ((4,) + block, like),
        ((2,) + block, like),
        (block, like),
        (block, like),
        (block, like),
        (block, like),
        ((4 * stride, features), like),
        (tokens.shape, like),
        ((experts, streams, 2 * HEAD_DIM, positions), like),
        ((streams, HEAD_DIM, query_lanes), like),
        ((4,) + att, like),
        ((2,) + att, like),
        (att, like),
        (att, like),
        ((streams, HEAD_DIM, query_lanes), f32),
        ((streams, 1, query_lanes), f32),
        ((streams, 1, query_lanes), f32),
        ((experts, tok_count), f32),
        (tokens.shape, f32),
        (out_weight.shape, like),
        (w_gate.shape, like),
        (w_up.shape, like),
        (w_down.shape, like),
    ]
    vmem = pl.BlockSpec(memory_space=pltpu.VMEM)
    hbm = pl.BlockSpec(memory_space=pl.ANY)
    return pl.pallas_call(
        functools.partial(fused_kernel, experts, capacity),
        out_shape=(jax.ShapeDtypeStruct(tokens.shape, like), jax.ShapeDtypeStruct(att, like)),
        in_specs=[vmem] * 11 + [hbm] * 4,
        out_specs=(vmem, vmem),
        scratch_shapes=[pltpu.VMEM(shape, dtype) for shape, dtype in shapes]
        + [pltpu.SemaphoreType.DMA((4,)), pltpu.SemaphoreType.DMA((2,))]
        + [sem] * 20
        + [pltpu.SemaphoreType.DMA((3,))] * 2,
        name="fused",
        compiler_params=pltpu.CompilerParams(
            collective_id=1, has_side_effects=True, vmem_limit_bytes=62 * 2**20
        ),
    )(tokens, moe_gain, routes, weights, queries, keys, values, q_gain, k_gain, cosine, sine,
      out_weight, w_gate, w_up, w_down)


def per_device(
    queries,
    keys,
    values,
    query_gain,
    key_gain,
    out_weight,
    moe_tokens,
    moe_gain,
    routes,
    route_weight,
    w_gate,
    w_up,
    w_down,
):
    pos_count, seq_count = queries.shape[:2]
    positions = lax.axis_index("ep") * pos_count + jnp.arange(pos_count, dtype=jnp.int32)
    inverse = THETA ** (-jnp.arange(QUARTER, dtype=jnp.float32) / QUARTER)
    grid_row = (positions // GRID_W).astype(jnp.float32)
    grid_col = (positions % GRID_W).astype(jnp.float32)
    angles = jnp.concatenate([inverse[:, None] * grid_row, inverse[:, None] * grid_col], axis=0)
    kv_local = keys.shape[2] // HEAD_DIM
    streams = seq_count * kv_local
    experts = lax.axis_size("ep")
    capacity = max(2, (3 * moe_tokens.shape[0] * routes.shape[1] + 2 * experts - 1) // (2 * experts))

    def by_feature(data):
        return jnp.transpose(data, (1, 2, 0)).reshape(streams, -1, pos_count)

    def wide(gain):
        return jnp.broadcast_to(gain[:, None], (HEAD_DIM, pos_count))

    routed, attended = fused(
        experts,
        capacity,
        moe_tokens,
        moe_gain[None, :],
        routes.T,
        route_weight.T,
        by_feature(queries),
        by_feature(keys),
        by_feature(values),
        wide(query_gain),
        wide(key_gain),
        jnp.cos(angles),
        jnp.sin(angles),
        out_weight,
        w_gate[0],
        w_up[0],
        w_down[0],
    )
    quarter = pos_count // lax.axis_size("tp")
    attended = jnp.transpose(attended.reshape(seq_count, quarter, -1), (1, 0, 2))
    return (attended, routed)


def solution(mesh):
    in_specs = (
        P("ep", None, "tp"),
        P("ep", None, "tp"),
        P("ep", None, "tp"),
        P(),
        P(),
        P("tp", None),
        P(("ep", "tp"), None),
        P(),
        P(("ep", "tp"), None),
        P(("ep", "tp"), None),
        P("ep", None, "tp"),
        P("ep", None, "tp"),
        P("ep", "tp", None),
    )
    out_specs = (P(("ep", "tp"), None, None), P(("ep", "tp"), None))
    return jax.shard_map(
        per_device, mesh=mesh, in_specs=in_specs, out_specs=out_specs, check_vma=False
    )
```

time: 128 us -> 135 us (1.055)
  the two profiles are of different devices: /device:TPU:0 before, /device:TPU:16 now
where the time goes in v1:
time: 135 us; the launch traced here: 133 us
  Pallas kernels  125 us (93%)
  local copies, waits for them, and re-layouts  6.82 us (5%)
    pallas_call x1, Pallas kernels, fused(): pl.pallas_call(functools.partial(fused_kernel, experts, capacity), out_sh...  125 us
    broadcast_in_dim x2, local copies, waits for them, and re-layouts, wide(): return jnp.broadcast_to(gain[:, None], (HEAD_DIM, pos_count))  2.71 us

profile of v1, /device:TPU:16, one launch (start us, length us, event | category | flops | bytes accessed | tf_op | source)
XLA Modules:
  0.0 133.3 jit_solution(17911718130164842526)
XLA Ops:
  0.6 0.0 copy-start.1
  0.7 0.1 broadcast_multiply_fusion.1
  0.8 0.8 fusion
  1.5 1.4 %broadcast_in_dim.7.q_gain = f32[64,256]{1,0:T(8,128)} broadcast(f32[64]{0:T(128)} %param.16), dimensions={0} | broadcast | bytes 65792 | tf_op jit(solution)/shard_map/broadcast_in_dim | solution.py:483
  2.9 1.4 %broadcast_in_dim.8.k_gain = f32[64,256]{1,0:T(8,128)} broadcast(f32[64]{0:T(128)} %param.17), dimensions={0} | broadcast | bytes 65792 | tf_op jit(solution)/shard_map/broadcast_in_dim | solution.py:483
  4.2 0.0 copy-done.1
  4.2 0.9 copy.15
  5.1 125.0 %fused.1 = (bf16[128,2048]{1,0:T(8,128)(2,1)}, bf16[128,2048]{1,0:T(8,128)(2,1)}) custom-call(bf16[128,2048]{1,0:T(8,128)(2,1)} %tokens.1, f32[1,2048]{1,0:T(1,128)} %bitcast.21, s32[2,128]{1,0:T(2,128)} %bitcast.22, f32[2,128]{1,0:T(2,128)} %bitcast.23, bf16[2,256,256]{2,1,0:T(8,128)(2,1)} %bitcast.16, bf16[2,64,256]{2,1,0:T(8,128)(2,1)} %bitcast.19, ...), custom_call_target="tpu_custom_call" | custom-call | tf_op jit(solution)/shard_map/fused/pallas_call | solution.py:436
  130.1 0.0 copy-start
  130.1 2.4 %copy.18 = bf16[2,64,2048]{2,0,1:T(2,128)(2,1)} copy(bf16[2,64,2048]{2,1,0:T(8,128)(2,1)} %bitcast.18) | data formatting | bytes 1048576 | tf_op jit(solution)/shard_map/reshape | solution.py:505
  132.5 0.0 copy-done
  132.5 0.8 copy.20
  (2 shorter events, 0.0 us)
Async XLA Ops:
  0.6 3.6 %copy-start.1 = (bf16[256,2,256]{2,1,0:T(2,128)(2,1)S(1)}, bf16[256,2,256]{2,1,0:T(2,128)(2,1)}, u32[]{:S(2)}) copy-start(bf16[256,2,256]{2,1,0:T(2,128)(2,1)} %param.13) | copy-start | bytes 786436
  130.1 2.4 %copy-start = (bf16[128,2048]{1,0:T(8,128)(2,1)S(1)}, bf16[128,2048]{1,0:T(8,128)(2,1)}, u32[]{:S(2)}) copy-start(bf16[128,2048]{1,0:T(8,128)(2,1)} %get-tuple-element.15) | copy-start | bytes 1572868

commit v2 on v1

--- a/solution.py
+++ b/solution.py
@@ -25,6 +25,20 @@
         result = result + (a // bit + b // bit) % 2 * bit
         bit *= 2
     return result
+
+
+def pick(place, special, rest):
+    for where, value in special:
+        rest = jnp.where(place == where, value, rest)
+    return rest
+
+
+def in_order(place):
+    return pick(place, ((3, 4), (4, 5), (5, 3)), place)
+
+
+def out_order(place, count):
+    return pick(place, ((0, 4), (1, 5), (2, 1), (count - 3, 2), (count - 2, 3), (count - 1, 0)), place + 3)
 
 
 def turned(block, gain, cosine, sine):
@@ -158,22 +172,13 @@
         return (slot == row).astype(f32)
 
     batch = min(experts, 4)
+    kv_at, attend_at = 5, 9
 
     def dispatch(g):
         table = jnp.concatenate([places(g * batch + i) for i in range(batch)], axis=0).astype(bf16)
         chosen = jnp.dot(table, normed[...], preferred_element_type=f32).astype(bf16)
         for i in range(batch):
             send[g * batch + i] = chosen[i * stride : i * stride + capacity]
-
-    def send_batch(g):
-        for i in range(batch):
-            if i == 0:
-
-                @pl.when(g > 0)
-                def _():
-                    chunk(g * batch).start()
-            else:
-                chunk(g * batch + i).start()
 
     def column(row):
         square = (tok_count, tok_count)
@@ -221,148 +226,150 @@
 
     pl.semaphore_wait(barrier, len(partners))
 
-    lax.fori_loop(1, half, lambda m, c: (kv_direct(m).start(), c)[1], 0)
-    kv_side(0).start()
-
-    def dispatch_step(g, carry):
-        @pl.when(g < experts // batch)
-        def _():
-            dispatch(g)
-
-        @pl.when(g > 0)
-        def _():
-            send_batch(g - 1)
-
-        @pl.when(g == experts // batch - 1)
-        def _():
-            for s in range(streams):
-                for h in range(groups):
-                    head = turned(queries[s, h * HEAD_DIM : (h + 1) * HEAD_DIM], q_gain[...], cosine[...], sine[...])
-                    q[s, :, h * positions : (h + 1) * positions] = head * bf16(HEAD_DIM**-0.5)
-
-        @pl.when(g == 1)
-        def _():
-            own_copy(0).start()
-
-        return carry
-
-    lax.fori_loop(0, experts // batch + 1, dispatch_step, 0)
+    lax.fori_loop(0, experts // batch, lambda g, c: (dispatch(g), c)[1], 0)
+    for s in range(streams):
+        for h in range(groups):
+            head = turned(queries[s, h * HEAD_DIM : (h + 1) * HEAD_DIM], q_gain[...], cosine[...], sine[...])
+            q[s, :, h * positions : (h + 1) * positions] = head * bf16(HEAD_DIM**-0.5)
+    own_copy(0).start()
+    for k in (1, 2, 4, 5):
+        chunk(k).start()
     best[...] = jnp.full_like(best, -1e30)
     total[...] = jnp.zeros_like(total)
     accum[...] = jnp.zeros_like(accum)
     combined[...] = jnp.zeros_like(combined)
     own_copy(0).wait()
-    across(0).start()
-    beside(0).start()
-
-    early = 2
-
-    def attention_step(m, carry):
-        attend(2 * m)
-
-        @pl.when(m + 1 < half)
-        def _():
-            kv_direct(m + 1).wait_recv()
-            kv_side(m + 1).start()
-
-        kv_side(m).wait_recv()
-        attend(2 * m + 1)
-
-        @pl.when(m == half - 3)
-        def _():
-            chunk(1).wait_recv()
-            across(1).start()
-            beside(1).start()
-
-        return carry
-
-    lax.fori_loop(0, half, attention_step, 0)
-    weight_copy(0).wait()
-    project()
-    for i in range(1, 4):
+    for i in range(4):
         weight_copy(i).wait()
 
-    def step(k, carry):
-        @pl.when((k >= early) & (k < experts))
-        def _():
-            chunk(k).wait_recv()
+    def step(i, carry):
+        def within(least, most):
+            return pl.when((i >= least) & (i < most))
+
+        def when_out(delay):
+            return within(delay, experts + delay)
+
+        def out(delay):
+            return out_order(i - delay, experts)
+
+        @within(0, experts)
+        def _():
+            k = in_order(i)
+
+            @pl.when(i > 0)
+            def _():
+                chunk(k).wait_recv()
+
             across(k).start()
             beside(k).start()
 
-        @pl.when((k >= 3) & (k < experts + 3))
-        def _():
-            pair_far(k - 3).start()
-            pair_near(k - 3).start()
-
-        @pl.when((k >= 5) & (k < experts + 5))
-        def _():
-            over(k - 5).start()
-
-        @pl.when((k >= 8) & (k < experts + 7))
-        def _():
-            back(k - 7).start()
-
-        @pl.when(k == 7)
-        def _():
-            own_copy(1).start()
-
-        @pl.when(k == 1)
-        def _():
-            other(1).start()
-            other(0).start()
-
-        @pl.when((k >= 1) & (k < experts + 1))
-        def _():
-            across(k - 1).wait_recv()
-            relay(k - 1).start()
-
-        @pl.when(k == 3)
-        def _():
-            other(2).start()
-
-        @pl.when((k >= 2) & (k < experts + 2))
-        def _():
-            beside(k - 2).wait_recv()
-            relay(k - 2).wait_recv()
-            expert(k - 2)
-
-        @pl.when(k == 2)
+            @pl.when(k == 2)
+            def _():
+                chunk(3).start()
+
+            @pl.when((k >= 4) & (k + 2 < experts))
+            def _():
+                chunk(k + 2).start()
+
+        @within(kv_at, kv_at + 1)
+        def _():
+            kv_side(0).start()
+            lax.fori_loop(1, half, lambda m, c: (kv_direct(m).start(), c)[1], 0)
+
+        @within(1, experts + 1)
+        def _():
+            k = in_order(i - 1)
+            across(k).wait_recv()
+            relay(k).start()
+
+        @when_out(5)
+        def _():
+            j = out(5)
+            beside(j).wait_recv()
+            relay(j).wait_recv()
+            expert(j)
+
+        @when_out(6)
+        def _():
+            j = out(6)
+            pair_far(j).wait_recv()
+            gone[j] = (part[high, j].astype(f32) + pair[1, j].astype(f32)).astype(bf16)
+
+        @within(attend_at + half + 1, attend_at + half + 2)
         def _():
             other(1).wait_recv()
             gone_att[...] = (prod[high].astype(f32) + pair_att[1].astype(f32)).astype(bf16)
 
-        @pl.when((k >= 4) & (k < experts + 4))
-        def _():
-            j = k - 4
-            pair_far(j).wait_recv()
-            gone[j] = (part[high, j].astype(f32) + pair[1, j].astype(f32)).astype(bf16)
-
-        @pl.when((k >= 6) & (k < experts + 6))
-        def _():
-            j = k - 6
+        @when_out(8)
+        def _():
+            j = out(8)
             pair_near(j).wait_recv()
             over(j).wait_recv()
             done[j] = (part[t, j].astype(f32) + pair[0, j].astype(f32) + seen[j].astype(f32)).astype(bf16)
 
-        @pl.when((k >= 10) & (k < experts + 9))
-        def _():
-            back(k - 9).wait_recv()
-            combine(k - 9)
-
-        @pl.when(k == 9)
+        @when_out(5)
+        def _():
+            pair_far(out(5)).start()
+            pair_near(out(5)).start()
+
+        @when_out(6)
+        def _():
+            over(out(6)).start()
+
+        @within(8, experts + 7)
+        def _():
+            back(out(8)).start()
+
+        @within(experts + 7, experts + 8)
+        def _():
+            own_copy(1).start()
+
+        @within(attend_at + half + 1, attend_at + half + 2)
+        def _():
+            other(2).start()
+
+        @within(attend_at - 1, attend_at + half - 2)
+        def _():
+            m = i - attend_at + 2
+            kv_direct(m).wait_recv()
+            kv_side(m).start()
+
+        @within(attend_at, attend_at + half)
+        def _():
+            m = i - attend_at
+            attend(2 * m)
+            kv_side(m).wait_recv()
+            attend(2 * m + 1)
+
+        @within(attend_at + half, attend_at + half + 1)
+        def _():
+            project()
+            other(1).start()
+            other(0).start()
+
+        return carry
+
+    lax.fori_loop(0, experts + 8, step, 0)
+
+    def gather(k, carry):
+        @pl.when(k == 0)
         def _():
             own_copy(1).wait()
-            combine(0)
-
-        @pl.when(k == experts + 1)
+
+        @pl.when(k > 0)
+        def _():
+            back(k).wait_recv()
+
+        @pl.when(k == 3)
         def _():
             other(0).wait_recv()
             other(2).wait_recv()
             att[...] = (prod[t].astype(f32) + pair_att[0].astype(f32) + seen_att[...].astype(f32)).astype(bf16)
 
+        combine(k)
         return carry
 
-    lax.fori_loop(0, experts + 9, step, 0)
+    lax.fori_loop(0, experts, gather, 0)
     routed[...] = combined[...].astype(bf16)
 
     def finish(k, carry):
@@ -375,8 +382,8 @@
 
         @pl.when(k >= 1)
         def _():
+            back(k).wait_send()
             chunk(k).wait_send()
-            back(k).wait_send()
 
         @pl.when(k < half)
         def _():

time: 135 us -> 110 us (0.81)
  Pallas kernels: 125 us -> 99.9 us
    pallas_call x1, Pallas kernels: 125 us -> 99.9 us  [fused(): pl.pallas_call(functools.partial(fused_kernel, experts, capacity), out_sh...]
where the time goes in v2:
time: 110 us; the launch traced here: 108 us
  Pallas kernels  99.9 us (91%)
  local copies, waits for them, and re-layouts  6.82 us (6%)
    pallas_call x1, Pallas kernels, fused(): pl.pallas_call(functools.partial(fused_kernel, experts, capacity), out_sh...  99.9 us
    broadcast_in_dim x2, local copies, waits for them, and re-layouts, wide(): return jnp.broadcast_to(gain[:, None], (HEAD_DIM, pos_count))  2.71 us
    reshape x1, local copies, waits for them, and re-layouts, per_device(): attended.reshape(seq_count, quarter, -1)  2.43 us

profile of v2, /device:TPU:16, one launch (start us, length us, event | category | flops | bytes accessed | tf_op | source)
XLA Modules:
  0.0 108.2 jit_solution(17344965413101710749)
XLA Ops:
  0.6 0.0 copy-start.1
  0.7 0.1 broadcast_multiply_fusion.1
  0.8 0.8 fusion
  1.5 1.4 %broadcast_in_dim.7.q_gain = f32[64,256]{1,0:T(8,128)} broadcast(f32[64]{0:T(128)} %param.16), dimensions={0} | broadcast | bytes 65792 | tf_op jit(solution)/shard_map/broadcast_in_dim | solution.py:490
  2.9 1.4 %broadcast_in_dim.8.k_gain = f32[64,256]{1,0:T(8,128)} broadcast(f32[64]{0:T(128)} %param.17), dimensions={0} | broadcast | bytes 65792 | tf_op jit(solution)/shard_map/broadcast_in_dim | solution.py:490
  4.2 0.0 copy-done.1
  4.2 0.9 copy.15
  5.1 99.9 %fused.1 = (bf16[128,2048]{1,0:T(8,128)(2,1)}, bf16[128,2048]{1,0:T(8,128)(2,1)}) custom-call(bf16[128,2048]{1,0:T(8,128)(2,1)} %tokens.1, f32[1,2048]{1,0:T(1,128)} %bitcast.21, s32[2,128]{1,0:T(2,128)} %bitcast.22, f32[2,128]{1,0:T(2,128)} %bitcast.23, bf16[2,256,256]{2,1,0:T(8,128)(2,1)} %bitcast.16, bf16[2,64,256]{2,1,0:T(8,128)(2,1)} %bitcast.19, ...), custom_call_target="tpu_custom_call" | custom-call | tf_op jit(solution)/shard_map/fused/pallas_call | solution.py:443
  105.0 0.0 copy-start
  105.0 2.4 %copy.18 = bf16[2,64,2048]{2,0,1:T(2,128)(2,1)} copy(bf16[2,64,2048]{2,1,0:T(8,128)(2,1)} %bitcast.18) | data formatting | bytes 1048576 | tf_op jit(solution)/shard_map/reshape | solution.py:512
  107.4 0.0 copy-done
  107.4 0.8 copy.20
  (2 shorter events, 0.0 us)
Async XLA Ops:
  0.6 3.6 %copy-start.1 = (bf16[256,2,256]{2,1,0:T(2,128)(2,1)S(1)}, bf16[256,2,256]{2,1,0:T(2,128)(2,1)}, u32[]{:S(2)}) copy-start(bf16[256,2,256]{2,1,0:T(2,128)(2,1)} %param.13) | copy-start | bytes 786436
  105.0 2.4 %copy-start = (bf16[128,2048]{1,0:T(8,128)(2,1)S(1)}, bf16[128,2048]{1,0:T(8,128)(2,1)}, u32[]{:S(2)}) copy-start(bf16[128,2048]{1,0:T(8,128)(2,1)} %get-tuple-element.15) | copy-start | bytes 1572868

commit v3 on v2

--- a/solution.py
+++ b/solution.py
@@ -27,18 +27,40 @@
     return result
 
 
-def pick(place, special, rest):
-    for where, value in special:
-        rest = jnp.where(place == where, value, rest)
-    return rest
-
-
-def in_order(place):
-    return pick(place, ((3, 4), (4, 5), (5, 3)), place)
-
-
-def out_order(place, count):
-    return pick(place, ((0, 4), (1, 5), (2, 1), (count - 3, 2), (count - 2, 3), (count - 1, 0)), place + 3)
+RANKS = "RSTLXDGPOQUBKVACJHI"
+
+
+def schedule(experts, near):
+    half = experts // 2
+    far = list(range(near, experts))
+    if near == 4 and experts == 8:
+        listed = (
+            "R1 K0 S5 T0", "R4 S6 Q0 U1", "X0 P0 G0 L4", "O0 V1 R5 S7", "V2 X4 P4 L1", "G4 O4 L5 X1",
+            "P1 A0 R6 S2", "U2 X5 P5 G5", "O5 D4 B4 V3", "A1 L6 G1 O1", "R7 S3 U3 X6", "P6 D5 B5 G6",
+            "O6 R2 L2 X2", "P2 G2 O2 L7", "X7 P7 A2 G7", "O7 D6 B6 R3", "L3 X3 P3 A3", "G3 O3 D7 B7",
+            "J0 D1 B1 H0", "I0 D2 B2 C4", "C5 D0 B0 D3", "B3 C6 C0 C1", "C7 C2 C3",
+        )
+        return [(word[0], int(word[1:])) for word in " ".join(listed).split()]
+    program = []
+    for i in range(experts + 5):
+        stages = (("R", 0), ("S", -2), ("L", 1), ("X", 2), ("D", 5), ("G", 3), ("P", 2), ("O", 3), ("B", 5))
+        for name, delay in stages:
+            if 0 <= i - delay < experts:
+                program.append((name, i - delay))
+    program.append(("K", 0))
+    program += [("V", m) for m in range(1, half)] + [("A", m) for m in range(half)]
+    return program + [("J", 0), ("H", 0), ("I", 0)] + [("C", k) for k in range(experts)]
+
+
+def in_slots(program):
+    tables, slot, last = {name: [] for name in RANKS}, 0, -1
+    for name, number in program:
+        rank = RANKS.index(name)
+        if rank <= last:
+            slot += 1
+        last = rank
+        tables[name].append((slot, number))
+    return tables, slot + 1
 
 
 def turned(block, gain, cosine, sine):
@@ -61,9 +83,10 @@
 ):
     (send, rows, part, pair, gone, seen, done, ret, packed, normed) = scratch[:10]
     (kv_all, q, prod, pair_att, gone_att, seen_att, accum, best, total, codes, combined) = scratch[10:21]
-    (out_weight, w_gate, w_up, w_down, w_sem, own) = scratch[21:27]
-    (a_send, a_recv, y_send, y_recv, l_send, l_recv, m_send, m_recv, k_send, k_recv, x_send, x_recv) = scratch[27:39]
-    (f_send, f_recv, n_send, n_recv, c_send, c_recv, b_send, b_recv, o_send, o_recv) = scratch[39:]
+    (out_weight, w_gate, w_up, w_down, passed, normed_high, codes_high, w_sem, own) = scratch[21:30]
+    (a_send, a_recv, y_send, y_recv, l_send, l_recv, m_send, m_recv, k_send, k_recv, x_send, x_recv) = scratch[30:42]
+    (f_send, f_recv, n_send, n_recv, c_send, c_recv, b_send, b_recv, o_send, o_recv) = scratch[42:52]
+    (p_send, p_recv, t_send, t_recv) = scratch[52:]
     f32, bf16 = jnp.float32, jnp.bfloat16
     e, t = lax.axis_index("ep"), lax.axis_index("tp")
     low, high = t + 1 - 2 * (t % 2), (t + 2) % 4
@@ -87,11 +110,21 @@
     def kv_direct(m):
         return remote(kv_all.at[0], kv_all.at[2 * m], k_send.at[m], k_recv.at[m], (peer(2 * m), t))
 
+    def kv_onward(m):
+        return remote(kv_all.at[half], kv_all.at[2 * m], k_send.at[m], k_recv.at[m], (peer(2 * m - half), t))
+
     def kv_side(m):
         return remote(kv_all.at[2 * m], kv_all.at[2 * m + 1], x_send.at[m], x_recv.at[m], (side, t))
 
     def chunk(k):
         return remote(send.at[k], rows.at[t, k], a_send.at[k], a_recv.at[k], (peer(k), t))
+
+    def passed_chunk(k):
+        return remote(passed.at[k], rows.at[high, k], p_send.at[k], p_recv.at[k], (peer(k), t))
+
+    def whole_block(i):
+        src, dst = ((normed, normed_high), (codes, codes_high))[i]
+        return remote(src, dst, t_send.at[i], t_recv.at[i], (e, high))
 
     def across(k):
         block = rows.at[t, k]
@@ -166,13 +199,14 @@
         for b in range(4):
             part[b, k] = result[b * stride : b * stride + capacity]
 
-    def places(k):
-        row = codes[pl.ds(peer(k), 1), :]
+    def places(k, table=codes):
+        row = table[pl.ds(peer(k), 1), :]
         slot = lax.broadcasted_iota(jnp.int32, (stride, tok_count), 0).astype(f32)
         return (slot == row).astype(f32)
 
     batch = min(experts, 4)
-    kv_at, attend_at = 5, 9
+    near = 4 if experts == 8 and 4 * capacity > tok_count else 0
+    far = experts - near
 
     def dispatch(g):
         table = jnp.concatenate([places(g * batch + i) for i in range(batch)], axis=0).astype(bf16)
@@ -180,8 +214,15 @@
         for i in range(batch):
             send[g * batch + i] = chosen[i * stride : i * stride + capacity]
 
+    def dispatch_high():
+        table = jnp.concatenate([places(i, codes_high) for i in range(near)], axis=0).astype(bf16)
+        chosen = jnp.dot(table, normed_high[...], preferred_element_type=f32).astype(bf16)
+        rows[high, 0] = chosen[:capacity]
+        for i in range(1, near):
+            passed[i] = chosen[i * stride : i * stride + capacity]
+
     def column(row):
-        square = (tok_count, tok_count)
+        square = (row.shape[1], row.shape[1])
         diagonal = lax.broadcasted_iota(jnp.int32, square, 0) == lax.broadcasted_iota(jnp.int32, square, 1)
         return jnp.sum(jnp.where(diagonal, row, 0.0), axis=1, keepdims=True)
 
@@ -206,10 +247,6 @@
     for device in partners:
         pl.semaphore_signal(barrier, inc=1, device_id=device, device_id_type=MESH)
 
-    for s in range(streams):
-        kv_all[0, s, :HEAD_DIM] = turned(keys[s], k_gain[...], cosine[...], sine[...])
-        kv_all[0, s, HEAD_DIM:] = values[s]
-
     if stride != capacity:
         packed[...] = jnp.zeros_like(packed)
     hits = jnp.zeros((experts, tok_count), f32)
@@ -224,167 +261,175 @@
     mean = jnp.mean(token_float * token_float, axis=-1, keepdims=True)
     normed[...] = (token_float * lax.rsqrt(mean + EPS) * moe_gain[...]).astype(bf16)
 
+    lax.fori_loop(0, experts // batch, lambda g, c: (dispatch(g), c)[1], 0)
+    own_copy(0).start()
     pl.semaphore_wait(barrier, len(partners))
 
-    lax.fori_loop(0, experts // batch, lambda g, c: (dispatch(g), c)[1], 0)
+    if near:
+        whole_block(1).start()
+        whole_block(0).start()
+        chunk(near).start()
+        chunk(1).start()
+    else:
+        chunk(1).start()
+    own_copy(0).wait()
+    if near:
+        beside(0).start()
+
+    k_column = column(k_gain[...])
+    for s in range(streams):
+        kv_all[0, s, :HEAD_DIM] = turned(keys[s], k_column, cosine[...], sine[...])
+        kv_all[0, s, HEAD_DIM:] = values[s]
+    q_column = column(q_gain[...])
     for s in range(streams):
         for h in range(groups):
-            head = turned(queries[s, h * HEAD_DIM : (h + 1) * HEAD_DIM], q_gain[...], cosine[...], sine[...])
+            head = turned(queries[s, h * HEAD_DIM : (h + 1) * HEAD_DIM], q_column, cosine[...], sine[...])
             q[s, :, h * positions : (h + 1) * positions] = head * bf16(HEAD_DIM**-0.5)
-    own_copy(0).start()
-    for k in (1, 2, 4, 5):
-        chunk(k).start()
     best[...] = jnp.full_like(best, -1e30)
     total[...] = jnp.zeros_like(total)
     accum[...] = jnp.zeros_like(accum)
     combined[...] = jnp.zeros_like(combined)
-    own_copy(0).wait()
     for i in range(4):
         weight_copy(i).wait()
 
+    def forward(k):
+        @pl.when(k > 0)
+        def _():
+            chunk(k).wait_recv()
+
+        beside(k).start()
+
+        @pl.when(k >= near)
+        def _():
+            across(k).start()
+
+    def block_arrived():
+        for i in range(2):
+            whole_block(i).wait_recv()
+        dispatch_high()
+
+    def onward(k):
+        @pl.when(k >= near)
+        def _():
+            across(k).wait_recv()
+
+        if near:
+
+            @pl.when(k < near)
+            def _():
+                passed_chunk(k).wait_recv()
+
+        relay(k).start()
+
+    def worked(k):
+        beside(k).wait_recv()
+        relay(k).wait_recv()
+        expert(k)
+
+    def pair_start(k):
+        pair_far(k).start()
+        pair_near(k).start()
+
+    def half_sum(k):
+        pair_far(k).wait_recv()
+        gone[k] = (part[high, k].astype(f32) + pair[1, k].astype(f32)).astype(bf16)
+
+    def whole_sum(k):
+        pair_near(k).wait_recv()
+        over(k).wait_recv()
+        done[k] = (part[t, k].astype(f32) + pair[0, k].astype(f32) + seen[k].astype(f32)).astype(bf16)
+
+    def back_start(k):
+        @pl.when(k > 0)
+        def _():
+            back(k).start()
+
+        @pl.when(k == 0)
+        def _():
+            own_copy(1).start()
+
+    def back_arrived(k):
+        @pl.when(k > 0)
+        def _():
+            back(k).wait_recv()
+
+        @pl.when(k == 0)
+        def _():
+            own_copy(1).wait()
+
+        combine(k)
+
+    def kv_start(_):
+        kv_side(0).start()
+        lax.fori_loop(1, half // 2 + 1, lambda m, c: (kv_direct(m).start(), c)[1], 0)
+
+    def kv_arrived(m):
+        kv_direct(m).wait_recv()
+        kv_side(m).start()
+
+        @pl.when(m == half // 2)
+        def _():
+            lax.fori_loop(half // 2 + 1, half, lambda i, c: (kv_onward(i).start(), c)[1], 0)
+
+    def attention(m):
+        attend(2 * m)
+        kv_side(m).wait_recv()
+        attend(2 * m + 1)
+
+    def projected(_):
+        project()
+        other(1).start()
+        other(0).start()
+
+    def other_half(_):
+        other(1).wait_recv()
+        gone_att[...] = (prod[high].astype(f32) + pair_att[1].astype(f32)).astype(bf16)
+
+    acts = dict(
+        R=forward, S=lambda k: chunk(k).start(), T=lambda _: block_arrived(), L=onward, X=worked, D=whole_sum,
+        G=half_sum, P=pair_start, O=lambda k: over(k).start(), Q=lambda _: relay(0).start(), U=lambda k: passed_chunk(k).start(), B=back_start, K=kv_start,
+        V=kv_arrived, A=attention, C=back_arrived, J=projected, H=other_half, I=lambda _: other(2).start(),
+    )
+    tables, slots = in_slots(schedule(experts, near))
+
     def step(i, carry):
-        def within(least, most):
-            return pl.when((i >= least) & (i < most))
-
-        def when_out(delay):
-            return within(delay, experts + delay)
-
-        def out(delay):
-            return out_order(i - delay, experts)
-
-        @within(0, experts)
-        def _():
-            k = in_order(i)
-
-            @pl.when(i > 0)
-            def _():
-                chunk(k).wait_recv()
-
-            across(k).start()
-            beside(k).start()
-
-            @pl.when(k == 2)
-            def _():
-                chunk(3).start()
-
-            @pl.when((k >= 4) & (k + 2 < experts))
-            def _():
-                chunk(k + 2).start()
-
-        @within(kv_at, kv_at + 1)
-        def _():
-            kv_side(0).start()
-            lax.fori_loop(1, half, lambda m, c: (kv_direct(m).start(), c)[1], 0)
-
-        @within(1, experts + 1)
-        def _():
-            k = in_order(i - 1)
-            across(k).wait_recv()
-            relay(k).start()
-
-        @when_out(5)
-        def _():
-            j = out(5)
-            beside(j).wait_recv()
-            relay(j).wait_recv()
-            expert(j)
-
-        @when_out(6)
-        def _():
-            j = out(6)
-            pair_far(j).wait_recv()
-            gone[j] = (part[high, j].astype(f32) + pair[1, j].astype(f32)).astype(bf16)
-
-        @within(attend_at + half + 1, attend_at + half + 2)
-        def _():
-            other(1).wait_recv()
-            gone_att[...] = (prod[high].astype(f32) + pair_att[1].astype(f32)).astype(bf16)
-
-        @when_out(8)
-        def _():
-            j = out(8)
-            pair_near(j).wait_recv()
-            over(j).wait_recv()
-            done[j] = (part[t, j].astype(f32) + pair[0, j].astype(f32) + seen[j].astype(f32)).astype(bf16)
-
-        @when_out(5)
-        def _():
-            pair_far(out(5)).start()
-            pair_near(out(5)).start()
-
-        @when_out(6)
-        def _():
-            over(out(6)).start()
-
-        @within(8, experts + 7)
-        def _():
-            back(out(8)).start()
-
-        @within(experts + 7, experts + 8)
-        def _():
-            own_copy(1).start()
-
-        @within(attend_at + half + 1, attend_at + half + 2)
-        def _():
-            other(2).start()
-
-        @within(attend_at - 1, attend_at + half - 2)
-        def _():
-            m = i - attend_at + 2
-            kv_direct(m).wait_recv()
-            kv_side(m).start()
-
-        @within(attend_at, attend_at + half)
-        def _():
-            m = i - attend_at
-            attend(2 * m)
-            kv_side(m).wait_recv()
-            attend(2 * m + 1)
-
-        @within(attend_at + half, attend_at + half + 1)
-        def _():
-            project()
-            other(1).start()
-            other(0).start()
+        for name in RANKS:
+            table = tables[name]
+            if not table:
+                continue
+            number = jnp.int32(-1)
+            for slot, value in table:
+                number = jnp.where(i == slot, value, number)
+
+            @pl.when(number >= 0)
+            def _(name=name, number=number):
+                acts[name](number)
 
         return carry
 
-    lax.fori_loop(0, experts + 8, step, 0)
-
-    def gather(k, carry):
-        @pl.when(k == 0)
-        def _():
-            own_copy(1).wait()
-
-        @pl.when(k > 0)
-        def _():
-            back(k).wait_recv()
-
-        @pl.when(k == 3)
-        def _():
-            other(0).wait_recv()
-            other(2).wait_recv()
-            att[...] = (prod[t].astype(f32) + pair_att[0].astype(f32) + seen_att[...].astype(f32)).astype(bf16)
-
-        combine(k)
-        return carry
-
-    lax.fori_loop(0, experts, gather, 0)
+    lax.fori_loop(0, slots, step, 0)
+    other(0).wait_recv()
+    other(2).wait_recv()
+    att[...] = (prod[t].astype(f32) + pair_att[0].astype(f32) + seen_att[...].astype(f32)).astype(bf16)
     routed[...] = combined[...].astype(bf16)
 
     def finish(k, carry):
-        across(k).wait_send()
         beside(k).wait_send()
         relay(k).wait_send()
         pair_far(k).wait_send()
         pair_near(k).wait_send()
         over(k).wait_send()
 
+        @pl.when(k >= near)
+        def _():
+            across(k).wait_send()
+
         @pl.when(k >= 1)
         def _():
             back(k).wait_send()
             chunk(k).wait_send()
 
+
         @pl.when(k < half)
         def _():
             kv_side(k).wait_send()
@@ -396,6 +441,11 @@
         return carry
 
     lax.fori_loop(0, experts, finish, 0)
+    if near:
+        for k in range(1, near):
+            passed_chunk(k).wait_send()
+        for i in range(2):
+            whole_block(i).wait_send()
     for i in range(3):
         other(i).wait_send()
 
@@ -437,6 +487,9 @@
         (w_gate.shape, like),
         (w_up.shape, like),
         (w_down.shape, like),
+        ((4, capacity, features), like),
+        (tokens.shape, like),
+        ((experts, tok_count), f32),
     ]
     vmem = pl.BlockSpec(memory_space=pltpu.VMEM)
     hbm = pl.BlockSpec(memory_space=pl.ANY)
@@ -448,7 +501,9 @@
         scratch_shapes=[pltpu.VMEM(shape, dtype) for shape, dtype in shapes]
         + [pltpu.SemaphoreType.DMA((4,)), pltpu.SemaphoreType.DMA((2,))]
         + [sem] * 20
-        + [pltpu.SemaphoreType.DMA((3,))] * 2,
+        + [pltpu.SemaphoreType.DMA((3,))] * 2
+        + [pltpu.SemaphoreType.DMA((4,))] * 2
+        + [pltpu.SemaphoreType.DMA((2,))] * 2,
         name="fused",
         compiler_params=pltpu.CompilerParams(
             collective_id=1, has_side_effects=True, vmem_limit_bytes=62 * 2**20
@@ -486,9 +541,6 @@
     def by_feature(data):
         return jnp.transpose(data, (1, 2, 0)).reshape(streams, -1, pos_count)
 
-    def wide(gain):
-        return jnp.broadcast_to(gain[:, None], (HEAD_DIM, pos_count))
-
     routed, attended = fused(
         experts,
         capacity,
@@ -499,8 +551,8 @@
         by_feature(queries),
         by_feature(keys),
         by_feature(values),
-        wide(query_gain),
-        wide(key_gain),
+        query_gain[None, :],
+        key_gain[None, :],
         jnp.cos(angles),
         jnp.sin(angles),
         out_weight,

time: 110 us -> 105 us (0.955); the launches traced: 108 us -> 105 us
  local copies, waits for them, and re-layouts: 6.82 us -> 5.04 us
  Pallas kernels: 99.9 us -> 98.5 us
    broadcast_in_dim x2 -> x0, local copies, waits for them, and re-layouts: 2.71 us -> none  [wide(): return jnp.broadcast_to(gain[:, None], (HEAD_DIM, pos_count))]
    pallas_call x1, Pallas kernels: 99.9 us -> 98.5 us  [fused(): pl.pallas_call(functools.partial(fused_kernel, experts, capacity), out_sh...]
    unnamed x6 -> x4, local copies, waits for them, and re-layouts: 1.68 us -> 2.61 us
where the time goes in v3:
time: 105 us
  Pallas kernels  98.5 us (94%)
  local copies, waits for them, and re-layouts  5.04 us (5%)
    pallas_call x1, Pallas kernels, fused(): pl.pallas_call(functools.partial(fused_kernel, experts, capacity), out_sh...  98.5 us
    unnamed x4, local copies, waits for them, and re-layouts  2.61 us
    reshape x1, local copies, waits for them, and re-layouts, per_device(): attended.reshape(seq_count, quarter, -1)  2.43 us

profile of v3, /device:TPU:16, one launch (start us, length us, event | category | flops | bytes accessed | tf_op | source)
XLA Modules:
  0.0 105.0 jit_solution(16244317994889119152)
XLA Ops:
  0.7 0.1 broadcast_multiply_fusion.1
  0.7 0.8 fusion
  1.5 1.8 %copy.15 = bf16[256,2,256]{0,2,1:T(8,128)(2,1)} copy(bf16[256,2,256]{2,1,0:T(2,128)(2,1)} %param.13) | data formatting | bytes 524288 | tf_op args[0]
  3.3 98.5 %fused.1 = (bf16[128,2048]{1,0:T(8,128)(2,1)}, bf16[128,2048]{1,0:T(8,128)(2,1)}) custom-call(bf16[128,2048]{1,0:T(8,128)(2,1)} %tokens.1, f32[1,2048]{1,0:T(1,128)} %bitcast.23, s32[2,128]{1,0:T(2,128)} %bitcast.24, f32[2,128]{1,0:T(2,128)} %bitcast.25, bf16[2,256,256]{2,1,0:T(8,128)(2,1)} %bitcast.18, bf16[2,64,256]{2,1,0:T(8,128)(2,1)} %bitcast.21, ...), custom_call_target="tpu_custom_call" | custom-call | tf_op jit(solution)/shard_map/fused/pallas_call | solution.py:496
  101.8 0.0 copy-start
  101.8 2.4 %copy.18 = bf16[2,64,2048]{2,0,1:T(2,128)(2,1)} copy(bf16[2,64,2048]{2,1,0:T(8,128)(2,1)} %bitcast.20) | data formatting | bytes 1048576 | tf_op jit(solution)/shard_map/reshape | solution.py:564
  104.2 0.0 copy-done
  104.2 0.8 copy.20
  (2 shorter events, 0.0 us)
Async XLA Ops:
  101.8 2.4 %copy-start = (bf16[128,2048]{1,0:T(8,128)(2,1)S(1)}, bf16[128,2048]{1,0:T(8,128)(2,1)}, u32[]{:S(2)}) copy-start(bf16[128,2048]{1,0:T(8,128)(2,1)} %get-tuple-element.15) | copy-start | bytes 1572868

commit v4 on v3

--- a/solution.py
+++ b/solution.py
@@ -1,4 +1,5 @@
 import functools
+import math
 import math
 
 import jax
@@ -27,7 +28,7 @@
     return result
 
 
-RANKS = "RSTLXDGPOQUBKVACJHI"
+RANKS = "RSTLXDGPOQUBKVACFJHI"
 
 
 def schedule(experts, near):
@@ -35,10 +36,10 @@
     far = list(range(near, experts))
     if near == 4 and experts == 8:
         listed = (
-            "R1 K0 S5 T0", "R4 S6 Q0 U1", "X0 P0 G0 L4", "O0 V1 R5 S7", "V2 X4 P4 L1", "G4 O4 L5 X1",
-            "P1 A0 R6 S2", "U2 X5 P5 G5", "O5 D4 B4 V3", "A1 L6 G1 O1", "R7 S3 U3 X6", "P6 D5 B5 G6",
-            "O6 R2 L2 X2", "P2 G2 O2 L7", "X7 P7 A2 G7", "O7 D6 B6 R3", "L3 X3 P3 A3", "G3 O3 D7 B7",
-            "J0 D1 B1 H0", "I0 D2 B2 C4", "C5 D0 B0 D3", "B3 C6 C0 C1", "C7 C2 C3",
+            "R1 K0 S5 T0", "R4 S6 Q0 U1", "V1 X0 P0 G0", "O0 L4 L1 X1", "P1 V2 G1 O1", "R5 S7 S2 U2",
+            "X4 P4 V3 G4", "O4 A0 L5 R6", "S3 U3 X5 P5", "A1 G5 O5 D4", "B4 R7 L6 A2", "X6 P6 D5 B5",
+            "G6 O6 R2 L2", "X2 P2 A3 G2", "O2 L7 X7 P7", "J0 G7 O7 D6", "B6 R3 L3 X3", "P3 H0 G3 O3",
+            "D7 B7 D1 B1", "I0 D2 B2 C4", "C5 D0 B0 D3", "B3 C6 C0 C1", "C2 C7 F0 C3",
         )
         return [(word[0], int(word[1:])) for word in " ".join(listed).split()]
     program = []
@@ -49,7 +50,7 @@
                 program.append((name, i - delay))
     program.append(("K", 0))
     program += [("V", m) for m in range(1, half)] + [("A", m) for m in range(half)]
-    return program + [("J", 0), ("H", 0), ("I", 0)] + [("C", k) for k in range(experts)]
+    return program + [("J", 0), ("H", 0), ("I", 0)] + [("C", k) for k in range(experts)] + [("F", 0)]
 
 
 def in_slots(program):
@@ -78,15 +79,16 @@
 
 
 def fused_kernel(
-    experts, capacity, tokens, moe_gain, routes, weights, queries, keys, values, q_gain, k_gain, cosine, sine,
+    experts, capacity, tokens, moe_gain, routes, weights, queries_hbm, keys_hbm, values_hbm, q_gain, k_gain,
     out_weight_hbm, w_gate_hbm, w_up_hbm, w_down_hbm, routed, att, *scratch
 ):
     (send, rows, part, pair, gone, seen, done, ret, packed, normed) = scratch[:10]
     (kv_all, q, prod, pair_att, gone_att, seen_att, accum, best, total, codes, combined) = scratch[10:21]
-    (out_weight, w_gate, w_up, w_down, passed, normed_high, codes_high, w_sem, own) = scratch[21:30]
-    (a_send, a_recv, y_send, y_recv, l_send, l_recv, m_send, m_recv, k_send, k_recv, x_send, x_recv) = scratch[30:42]
-    (f_send, f_recv, n_send, n_recv, c_send, c_recv, b_send, b_recv, o_send, o_recv) = scratch[42:52]
-    (p_send, p_recv, t_send, t_recv) = scratch[52:]
+    (out_weight, w_gate, w_up, w_down, passed, normed_high, codes_high) = scratch[21:28]
+    (queries, keys, values, w_sem, own) = scratch[28:33]
+    (a_send, a_recv, y_send, y_recv, l_send, l_recv, m_send, m_recv, k_send, k_recv, x_send, x_recv) = scratch[33:45]
+    (f_send, f_recv, n_send, n_recv, c_send, c_recv, b_send, b_recv, o_send, o_recv) = scratch[45:55]
+    (p_send, p_recv, t_send, t_recv) = scratch[55:]
     f32, bf16 = jnp.float32, jnp.bfloat16
     e, t = lax.axis_index("ep"), lax.axis_index("tp")
     low, high = t + 1 - 2 * (t % 2), (t + 2) % 4
@@ -161,7 +163,8 @@
         return pltpu.make_async_copy(done.at[0], ret.at[0], own.at[1])
 
     def weight_copy(i):
-        pairs = ((out_weight_hbm, out_weight), (w_gate_hbm, w_gate), (w_up_hbm, w_up), (w_down_hbm, w_down))
+        pairs = ((keys_hbm, keys), (values_hbm, values), (queries_hbm, queries), (out_weight_hbm, out_weight))
+        pairs += ((w_gate_hbm, w_gate), (w_up_hbm, w_up), (w_down_hbm, w_down))
         return pltpu.make_async_copy(pairs[i][0], pairs[i][1], w_sem.at[i])
 
     def attend(j):
@@ -179,14 +182,19 @@
             accum[s] = accum[s] * factor + added
 
     def project():
-        quarter = positions // 4
+        rows_out = positions * streams
+        place = lax.broadcasted_iota(jnp.int32, (positions, rows_out), 1)
+        position = lax.broadcasted_iota(jnp.int32, (positions, rows_out), 0)
+        laid = jnp.zeros((groups * HEAD_DIM, rows_out), f32)
         for s in range(streams):
             mixed = (accum[s] / total[s]).astype(bf16)
             stacked = jnp.concatenate([mixed[:, g * positions : (g + 1) * positions] for g in range(groups)], axis=0)
-            product = lax.dot_general(stacked, out_weight[...], (((0,), (0,)), ((), ())), preferred_element_type=f32)
-            product = product.astype(bf16)
-            for b in range(4):
-                prod[b, s * quarter : (s + 1) * quarter, :] = product[b * quarter : (b + 1) * quarter]
+            chosen = (place == position * streams + s).astype(f32).astype(bf16)
+            laid = laid + jnp.dot(stacked, chosen, preferred_element_type=f32)
+        for b in range(4):
+            block = laid[:, b * rows_out // 4 : (b + 1) * rows_out // 4].astype(bf16)
+            product = lax.dot_general(block, out_weight[...], (((0,), (0,)), ((), ())), preferred_element_type=f32)
+            prod[b] = product.astype(bf16)
 
     def expert(k):
         for b in range(4):
@@ -240,7 +248,7 @@
             weight_row = weight_row + jnp.where(routes[c : c + 1] == expert_id, weights[c : c + 1], 0.0)
         combined[...] += picked * column(weight_row)
 
-    for i in range(4):
+    for i in range(7):
         weight_copy(i).start()
     barrier = pltpu.get_barrier_semaphore()
     partners = [(peer(k), t) for k in range(1, experts)] + [(e, low), (e, high)]
@@ -276,20 +284,34 @@
     if near:
         beside(0).start()
 
+    for i in range(3):
+        weight_copy(i).wait()
+    shape = (2 * QUARTER, positions)
+    turn_row = lax.broadcasted_iota(jnp.int32, shape, 0)
+    power = (turn_row % QUARTER).astype(f32) * (-math.log(THETA) / QUARTER)
+    place = e * positions + lax.broadcasted_iota(jnp.int32, shape, 1)
+    grid = jnp.where(turn_row < QUARTER, place // GRID_W, place % GRID_W).astype(f32)
+    angles = grid * jnp.exp(power)
+    cosine, sine = jnp.cos(angles), jnp.sin(angles)
     k_column = column(k_gain[...])
     for s in range(streams):
-        kv_all[0, s, :HEAD_DIM] = turned(keys[s], k_column, cosine[...], sine[...])
+        kv_all[0, s, :HEAD_DIM] = turned(keys[s], k_column, cosine, sine)
         kv_all[0, s, HEAD_DIM:] = values[s]
     q_column = column(q_gain[...])
+    flat = queries[...].reshape(positions * streams, groups * HEAD_DIM)
+    row = lax.broadcasted_iota(jnp.int32, (positions * streams, positions), 0)
+    position = lax.broadcasted_iota(jnp.int32, (positions * streams, positions), 1)
     for s in range(streams):
+        chosen = (row == position * streams + s).astype(f32).astype(bf16)
+        by_feature = lax.dot_general(flat, chosen, (((0,), (0,)), ((), ())), preferred_element_type=f32)
         for h in range(groups):
-            head = turned(queries[s, h * HEAD_DIM : (h + 1) * HEAD_DIM], q_column, cosine[...], sine[...])
+            head = turned(by_feature[h * HEAD_DIM : (h + 1) * HEAD_DIM], q_column, cosine, sine)
             q[s, :, h * positions : (h + 1) * positions] = head * bf16(HEAD_DIM**-0.5)
     best[...] = jnp.full_like(best, -1e30)
     total[...] = jnp.zeros_like(total)
     accum[...] = jnp.zeros_like(accum)
     combined[...] = jnp.zeros_like(combined)
-    for i in range(4):
+    for i in range(3, 7):
         weight_copy(i).wait()
 
     def forward(k):
@@ -385,10 +407,16 @@
         other(1).wait_recv()
         gone_att[...] = (prod[high].astype(f32) + pair_att[1].astype(f32)).astype(bf16)
 
+    def finish_attended(_):
+        other(0).wait_recv()
+        other(2).wait_recv()
+        summed = prod[t].astype(f32) + pair_att[0].astype(f32) + seen_att[...].astype(f32)
+        att[...] = summed.astype(bf16).reshape(att.shape)
+
     acts = dict(
         R=forward, S=lambda k: chunk(k).start(), T=lambda _: block_arrived(), L=onward, X=worked, D=whole_sum,
         G=half_sum, P=pair_start, O=lambda k: over(k).start(), Q=lambda _: relay(0).start(), U=lambda k: passed_chunk(k).start(), B=back_start, K=kv_start,
-        V=kv_arrived, A=attention, C=back_arrived, J=projected, H=other_half, I=lambda _: other(2).start(),
+        V=kv_arrived, A=attention, C=back_arrived, J=projected, H=other_half, I=lambda _: other(2).start(), F=finish_attended,
     )
     tables, slots = in_slots(schedule(experts, near))
 
@@ -408,9 +436,6 @@
         return carry
 
     lax.fori_loop(0, slots, step, 0)
-    other(0).wait_recv()
-    other(2).wait_recv()
-    att[...] = (prod[t].astype(f32) + pair_att[0].astype(f32) + seen_att[...].astype(f32)).astype(bf16)
     routed[...] = combined[...].astype(bf16)
 
     def finish(k, carry):
@@ -451,14 +476,15 @@
 
 
 def fused(experts, capacity, tokens, moe_gain, routes, weights, queries, keys, *rest):
-    values, q_gain, k_gain, cosine, sine, out_weight, w_gate, w_up, w_down = rest
+    values, q_gain, k_gain, out_weight, w_gate, w_up, w_down = rest
     like = tokens.dtype
     f32 = jnp.float32
     sem = pltpu.SemaphoreType.DMA((experts,))
     tok_count, features = tokens.shape
     streams, _, positions = keys.shape
-    query_lanes = queries.shape[1] // HEAD_DIM * positions
+    query_lanes = queries.shape[2] // HEAD_DIM * positions
     att = (positions // 4 * streams, features)
+    att_out = (positions // 4, streams, features)
     stride = -(-capacity // 16) * 16
     block = (experts, capacity, features)
     shapes = [
@@ -490,16 +516,19 @@
         ((4, capacity, features), like),
         (tokens.shape, like),
         ((experts, tok_count), f32),
+        (queries.shape, like),
+        (keys.shape, like),
+        (values.shape, like),
     ]
     vmem = pl.BlockSpec(memory_space=pltpu.VMEM)
     hbm = pl.BlockSpec(memory_space=pl.ANY)
     return pl.pallas_call(
         functools.partial(fused_kernel, experts, capacity),
-        out_shape=(jax.ShapeDtypeStruct(tokens.shape, like), jax.ShapeDtypeStruct(att, like)),
-        in_specs=[vmem] * 11 + [hbm] * 4,
+        out_shape=(pltpu.VMEM(tokens.shape, like), pltpu.VMEM(att_out, like)),
+        in_specs=[vmem] * 4 + [hbm] * 3 + [vmem] * 2 + [hbm] * 4,
         out_specs=(vmem, vmem),
         scratch_shapes=[pltpu.VMEM(shape, dtype) for shape, dtype in shapes]
-        + [pltpu.SemaphoreType.DMA((4,)), pltpu.SemaphoreType.DMA((2,))]
+        + [pltpu.SemaphoreType.DMA((7,)), pltpu.SemaphoreType.DMA((2,))]
         + [sem] * 20
         + [pltpu.SemaphoreType.DMA((3,))] * 2
         + [pltpu.SemaphoreType.DMA((4,))] * 2
@@ -508,8 +537,28 @@
         compiler_params=pltpu.CompilerParams(
             collective_id=1, has_side_effects=True, vmem_limit_bytes=62 * 2**20
         ),
-    )(tokens, moe_gain, routes, weights, queries, keys, values, q_gain, k_gain, cosine, sine,
+    )(tokens, moe_gain, routes, weights, queries, keys, values, q_gain, k_gain,
       out_weight, w_gate, w_up, w_down)
+
+
+def carry_kernel(*refs):
+    leave = [pltpu.make_async_copy(refs[i], refs[2 + i], refs[4].at[i]) for i in range(2)]
+    for copy in leave:
+        copy.start()
+    for copy in leave:
+        copy.wait()
+
+
+def carry(*arrays):
+    shapes = [jax.ShapeDtypeStruct(array.shape, array.dtype) for array in arrays]
+    return pl.pallas_call(
+        carry_kernel,
+        out_shape=tuple(shapes),
+        in_specs=[pl.BlockSpec(memory_space=pltpu.VMEM)] * 2,
+        out_specs=(pl.BlockSpec(memory_space=pl.ANY),) * 2,
+        scratch_shapes=[pltpu.SemaphoreType.DMA((2,))],
+        name="carry",
+    )(*[pltpu.with_memory_space_constraint(array, pltpu.VMEM) for array in arrays])
 
 
 def per_device(
@@ -528,11 +577,6 @@
     w_down,
 ):
     pos_count, seq_count = queries.shape[:2]
-    positions = lax.axis_index("ep") * pos_count + jnp.arange(pos_count, dtype=jnp.int32)
-    inverse = THETA ** (-jnp.arange(QUARTER, dtype=jnp.float32) / QUARTER)
-    grid_row = (positions // GRID_W).astype(jnp.float32)
-    grid_col = (positions % GRID_W).astype(jnp.float32)
-    angles = jnp.concatenate([inverse[:, None] * grid_row, inverse[:, None] * grid_col], axis=0)
     kv_local = keys.shape[2] // HEAD_DIM
     streams = seq_count * kv_local
     experts = lax.axis_size("ep")
@@ -548,21 +592,17 @@
         moe_gain[None, :],
         routes.T,
         route_weight.T,
-        by_feature(queries),
+        queries,
         by_feature(keys),
         by_feature(values),
         query_gain[None, :],
         key_gain[None, :],
-        jnp.cos(angles),
-        jnp.sin(angles),
         out_weight,
         w_gate[0],
         w_up[0],
         w_down[0],
     )
-    quarter = pos_count // lax.axis_size("tp")
-    attended = jnp.transpose(attended.reshape(seq_count, quarter, -1), (1, 0, 2))
-    return (attended, routed)
+    return carry(attended, routed)
 
 
 def solution(mesh):

time: 105 us -> 97.2 us (0.926)
  local copies, waits for them, and re-layouts: 5.04 us -> 0 us
  Pallas kernels: 98.5 us -> 95.5 us
    pallas_call x1, Pallas kernels: 98.5 us -> 94.5 us  [fused(): pl.pallas_call(functools.partial(fused_kernel, experts, capacity), out_sh...]
    unnamed x4 -> x0, local copies, waits for them, and re-layouts: 2.61 us -> none
    reshape x1 -> x0, local copies, waits for them, and re-layouts: 2.43 us -> none  [per_device(): attended.reshape(seq_count, quarter, -1)]
where the time goes in v4:
time: 97.2 us; the launch traced here: 96.2 us
  Pallas kernels  95.5 us (98%)
    pallas_call x1, Pallas kernels, fused(): pl.pallas_call(functools.partial(fused_kernel, experts, capacity), out_sh...  94.5 us

profile of v4, /device:TPU:16, one launch (start us, length us, event | category | flops | bytes accessed | tf_op | source)
XLA Modules:
  0.0 96.2 jit_solution(7085238467802720720)
XLA Ops:
  0.6 94.5 %fused.1 = (bf16[128,2048]{1,0:T(8,128)(2,1)S(1)}, bf16[64,2,2048]{2,1,0:T(2,128)(2,1)S(1)}) custom-call(bf16[128,2048]{1,0:T(8,128)(2,1)} %tokens.1, f32[1,2048]{1,0:T(1,128)} %bitcast.15, s32[2,128]{1,0:T(2,128)} %bitcast.16, f32[2,128]{1,0:T(2,128)} %bitcast.17, bf16[256,2,256]{2,1,0:T(2,128)(2,1)} %queries_hbm.1, bf16[2,64,256]{2,1,0:T(8,128)(2,1)} %bitcast.13, ...), custom_call_target="tpu_custom_call" | custom-call | tf_op jit(solution)/shard_map/fused/pallas_call | solution.py:525
  95.2 1.0 %carry.1 = (bf16[64,2,2048]{2,1,0:T(2,128)(2,1)}, bf16[128,2048]{1,0:T(8,128)(2,1)}) custom-call(bf16[64,2,2048]{2,1,0:T(2,128)(2,1)S(1)} %get-tuple-element.4.refs_0_, bf16[128,2048]{1,0:T(8,128)(2,1)S(1)} %get-tuple-element.5.refs_1_), custom_call_target="tpu_custom_call" | custom-call | tf_op jit(solution)/shard_map/carry/pallas_call | solution.py:554

commit v5 on v4

--- a/solution.py
+++ b/solution.py
@@ -36,10 +36,10 @@
     far = list(range(near, experts))
     if near == 4 and experts == 8:
         listed = (
-            "R1 K0 S5 T0", "R4 S6 Q0 U1", "V1 X0 P0 G0", "O0 L4 L1 X1", "P1 V2 G1 O1", "R5 S7 S2 U2",
-            "X4 P4 V3 G4", "O4 A0 L5 R6", "S3 U3 X5 P5", "A1 G5 O5 D4", "B4 R7 L6 A2", "X6 P6 D5 B5",
-            "G6 O6 R2 L2", "X2 P2 A3 G2", "O2 L7 X7 P7", "J0 G7 O7 D6", "B6 R3 L3 X3", "P3 H0 G3 O3",
-            "D7 B7 D1 B1", "I0 D2 B2 C4", "C5 D0 B0 D3", "B3 C6 C0 C1", "C2 C7 F0 C3",
+            "R1 K0 T0 R4", "S5 Q0 U1 V1", "X0 P0 G0 O0", "L4 S6 L1 X1", "P1 V2 G1 O1", "S2 U2 X4 R5",
+            "S7 P4 G4 V3", "O4 A0 L5 R6", "S3 U3 X5 P5", "A1 G5 O5 D4", "B4 D1 B1 D0", "B0 R7 L6 A2",
+            "X6 P6 D5 B5", "G6 O6 R2 L2", "X2 P2 A3 G2", "O2 L7 X7 P7", "J0 G7 O7 D6", "B6 R3 L3 X3",
+            "P3 H0 G3 O3", "D7 B7 I0 D2", "B2 C4 C5 D3", "B3 C6 C0 C1", "C2 C7 F0 C3",
         )
         return [(word[0], int(word[1:])) for word in " ".join(listed).split()]
     program = []

time: 97.2 us -> 91.9 us (0.945)
  Pallas kernels: 95.5 us -> 90.4 us
    pallas_call x1, Pallas kernels: 94.5 us -> 89.4 us  [fused(): pl.pallas_call(functools.partial(fused_kernel, experts, capacity), out_sh...]
where the time goes in v5:
time: 91.9 us; the launch traced here: 91.1 us
  Pallas kernels  90.4 us (98%)
    pallas_call x1, Pallas kernels, fused(): pl.pallas_call(functools.partial(fused_kernel, experts, capacity), out_sh...  89.4 us

profile of v5, /device:TPU:16, one launch (start us, length us, event | category | flops | bytes accessed | tf_op | source)
XLA Modules:
  0.0 91.1 jit_solution(2822123845247028932)
XLA Ops:
  0.6 89.4 %fused.1 = (bf16[128,2048]{1,0:T(8,128)(2,1)S(1)}, bf16[64,2,2048]{2,1,0:T(2,128)(2,1)S(1)}) custom-call(bf16[128,2048]{1,0:T(8,128)(2,1)} %tokens.1, f32[1,2048]{1,0:T(1,128)} %bitcast.15, s32[2,128]{1,0:T(2,128)} %bitcast.16, f32[2,128]{1,0:T(2,128)} %bitcast.17, bf16[256,2,256]{2,1,0:T(2,128)(2,1)} %queries_hbm.1, bf16[2,64,256]{2,1,0:T(8,128)(2,1)} %bitcast.13, ...), custom_call_target="tpu_custom_call" | custom-call | tf_op jit(solution)/shard_map/fused/pallas_call | solution.py:525
  90.1 1.0 %carry.1 = (bf16[64,2,2048]{2,1,0:T(2,128)(2,1)}, bf16[128,2048]{1,0:T(8,128)(2,1)}) custom-call(bf16[64,2,2048]{2,1,0:T(2,128)(2,1)S(1)} %get-tuple-element.4.refs_0_, bf16[128,2048]{1,0:T(8,128)(2,1)S(1)} %get-tuple-element.5.refs_1_), custom_call_target="tpu_custom_call" | custom-call | tf_op jit(solution)/shard_map/carry/pallas_call | solution.py:554
